TPU v7x, 128 devices: a whole 4x4x4 slice. The times are simulated.
128 devices in a mesh: sp: 16 (over z, x), tp: 8 (over y, core).
Axes of the slice: x: 4, y: 4, z: 4, core: 2. Of those that a mesh axis runs over, the one named last changes fastest.
Arguments:
- query_small: bfloat16 [12288, 1024], P('sp', 'tp'), may hold values from -18 to 18
- key_small: bfloat16 [12288, 1024], P('sp', 'tp'), may hold values from -6 to 6
- value_small: bfloat16 [12288, 1024], P('sp', 'tp'), may hold values from -6 to 6
- offset_small: bfloat16 [16, 12288], P('tp', 'sp'), may hold values from -25 to 0
- query_large: bfloat16 [12288, 1024], P('sp', 'tp'), may hold values from -18 to 18
- key_large: bfloat16 [12288, 1024], P('sp', 'tp'), may hold values from -6 to 6
- value_large: bfloat16 [12288, 1024], P('sp', 'tp'), may hold values from -6 to 6
- offset_large: bfloat16 [8, 12288], P('tp', 'sp'), may hold values from -25 to 0
- out_small: bfloat16 [1024, 2048], P('tp'), may hold values from -0.125 to 0.125
- out_large: bfloat16 [1024, 2048], P('tp'), may hold values from -0.125 to 0.125
- residual: bfloat16 [12288, 2048], P(('sp', 'tp')), may hold values from -1.1953125 to 1.1953125
- norm_gain: bfloat16 [2048], replicated, may hold values from 0.099609375 to 1.8984375
- gate_weight: bfloat16 [2048, 5632], P('sp', 'tp'), may hold values from -0.125 to 0.125
- up_weight: bfloat16 [2048, 5632], P('sp', 'tp'), may hold values from -0.125 to 0.125
- down_weight: bfloat16 [5632, 2048], P('tp', 'sp'), may hold values from -0.078125 to 0.078125
Outputs:
- layer_out: bfloat16 [12288, 2048], P(('sp', 'tp'))
All inputs are finite; a program needn't handle non-finite values.
Results may differ from a plain program's by a relative error of at most 0.023.
Values may be sent and summed in bfloat16 or wider, within the bound.
A program may use at most 128 MiB of HBM per device.

v0:
```python
import jax
import jax.numpy as jnp
from jax import lax
from jax.sharding import PartitionSpec as P

SMALL_DIM = 64
LARGE_DIM = 128


def turned_gather(arrays, axis, dims):
    turned = [jnp.moveaxis(a, dim, 0) for a, dim in zip(arrays, dims)]
    both = jnp.concatenate([t.reshape(len(t), -1) for t in turned], axis=1)
    whole, at, done = (lax.all_gather(both, axis, axis=0, tiled=True), 0, [])
    for t, dim in zip(turned, dims):
        share = whole[:, at : at + t[0].size].reshape(-1, *t.shape[1:])
        done.append(jnp.moveaxis(share, 0, dim))
        at += t[0].size
    return tuple(done)


def cut_along(value, dim, length):
    before, after = (value.shape[:dim], value.shape[dim + 1 :])
    return jnp.moveaxis(value.reshape(*before, length, -1, *after), dim, 0)


def summed_on_arrival(value, axis, dim):
    pieces = cut_along(value, dim, lax.axis_size(axis))
    arrived = lax.all_to_all(pieces, axis, split_axis=0, concat_axis=0, tiled=True)
    return arrived.astype(jnp.float32).sum(axis=0)


def split_heads(flat, head_depth):
    return flat.reshape(flat.shape[0], -1, head_depth)


def stick_terms(query, random_keys, values, offset, limits, carried):
    head_depth = query.shape[-1]
    key_heads = split_heads(random_keys, head_depth)
    value_heads = split_heads(values, head_depth)
    logits = jnp.einsum(
        "thd,shd->hts", query, key_heads, preferred_element_type=jnp.float32
    ) * head_depth ** (-0.5)
    logits = logits + offset.astype(jnp.float32)[:, None, :]
    fail_all = jax.nn.log_sigmoid(-logits)
    log_pass = logits + fail_all
    log_fail = fail_all
    before = None
    if limits is not None:
        query_first, key_first = limits
        query_pos = lax.broadcasted_iota(jnp.int32, logits.shape, 1) + query_first
        key_pos = lax.broadcasted_iota(jnp.int32, logits.shape, 2) + key_first
        before = key_pos < query_pos
        log_fail = jnp.where(before, fail_all, 0.0)
    suffix = lax.cumsum(log_fail, axis=2, reverse=True) - log_fail
    weights = jnp.exp(log_pass + suffix + carried[:, :, None])
    if before is not None:
        weights = jnp.where(before, weights, 0.0)
    weights = weights.astype(jnp.bfloat16)
    result = jnp.einsum("hts,shd->thd", weights, value_heads, preferred_element_type=jnp.float32)
    return (result, carried + jnp.sum(log_fail, axis=2))


def both_groups(queries, key_block, limits, totals):
    key_small, value_small, offset_small, key_large, value_large, offset_large = key_block
    out_small, acc_small, out_large, acc_large = totals
    term_small, next_small = stick_terms(
        queries[0], key_small, value_small, offset_small, limits, acc_small
    )
    term_large, next_large = stick_terms(
        queries[1], key_large, value_large, offset_large, limits, acc_large
    )
    return (out_small + term_small, next_small, out_large + term_large, next_large)


def empty_totals(rows, small_heads, large_heads):
    return (
        jnp.zeros((rows, small_heads, SMALL_DIM), jnp.float32),
        jnp.zeros((small_heads, rows), jnp.float32),
        jnp.zeros((rows, large_heads, LARGE_DIM), jnp.float32),
        jnp.zeros((large_heads, rows), jnp.float32),
    )


def rounded(value):
    return lax.optimization_barrier(value.astype(jnp.bfloat16)).astype(jnp.float32)


def rms_norm(stream, gain):
    scale = lax.rsqrt(jnp.mean(stream * stream, axis=-1, keepdims=True) + 1e-06)
    return (stream * scale * gain.astype(jnp.float32)).astype(jnp.bfloat16)


def on_device(
    query_small,
    key_small,
    value_small,
    offset_small,
    query_large,
    key_large,
    value_large,
    offset_large,
    out_small,
    out_large,
    residual,
    norm_gain,
    gate_weight,
    up_weight,
    down_weight,
):
    gate_full, up_full, down_full = turned_gather(
        (gate_weight, up_weight, down_weight), "sp", (0, 0, 1)
    )
    tokens = query_small.shape[0]
    small_heads = offset_small.shape[0]
    large_heads = offset_large.shape[0]
    queries = (split_heads(query_small, SMALL_DIM), split_heads(query_large, LARGE_DIM))
    own_block = (key_small, value_small, offset_small, key_large, value_large, offset_large)
    sp_index = lax.axis_index("sp")
    own_start = sp_index * tokens
    totals = both_groups(
        queries, own_block, (own_start, own_start), empty_totals(tokens, small_heads, large_heads)
    )
    key_dims = (0, 0, 1, 0, 0, 1)
    gathered = turned_gather(
        (own_block[0], own_block[1], own_block[2], own_block[3], own_block[4], own_block[5]),
        "sp",
        (0, 0, 1, 0, 0, 1),
    )

    def far_turn(turn_index, status):
        first_row = (sp_index - 1 - turn_index) * tokens
        key_block = tuple(
            (
                lax.dynamic_slice_in_dim(member, first_row, tokens, member_dim)
                for member, member_dim in zip(gathered, key_dims)
            )
        )
        return both_groups(queries, key_block, None, status)

    totals = lax.fori_loop(0, sp_index, far_turn, totals)
    mixed_small = totals[0].reshape(tokens, -1).astype(jnp.bfloat16)
    mixed_large = totals[2].reshape(tokens, -1).astype(jnp.bfloat16)
    attended = summed_on_arrival(
        (
            jnp.dot(mixed_small, out_small, preferred_element_type=jnp.float32)
            + jnp.dot(mixed_large, out_large, preferred_element_type=jnp.float32)
        ).astype(jnp.bfloat16),
        "tp",
        0,
    )
    stream = residual.astype(jnp.float32) + rounded(attended)
    normed = rms_norm(stream, norm_gain)
    normed_rows = lax.all_gather(normed, "tp", axis=0, tiled=True)
    gate = jnp.dot(normed_rows, gate_full, preferred_element_type=jnp.float32)
    upper = jnp.dot(normed_rows, up_full, preferred_element_type=jnp.float32)
    hidden = (jax.nn.silu(gate) * upper).astype(jnp.bfloat16)
    summed = lax.psum_scatter(
        jnp.dot(hidden, down_full, preferred_element_type=jnp.float32).astype(jnp.bfloat16),
        "tp",
        scatter_dimension=0,
        tiled=True,
    ).astype(jnp.float32)
    return (stream + rounded(summed)).astype(jnp.bfloat16)


def solution(mesh):
    return jax.shard_map(
        on_device,
        mesh=mesh,
        in_specs=(
            P("sp", "tp"),
            P("sp", "tp"),
            P("sp", "tp"),
            P("tp", "sp"),
            P("sp", "tp"),
            P("sp", "tp"),
            P("sp", "tp"),
            P("tp", "sp"),
            P("tp", None),
            P("tp", None),
            P(("sp", "tp"), None),
            P(),
            P("sp", "tp"),
            P("sp", "tp"),
            P("tp", "sp"),
        ),
        out_specs=P(("sp", "tp"), None),
        check_vma=False,
    )
```

profile of v0, /device:TPU:96, one launch (start us, length us, event | category | flops | bytes accessed | tf_op | source)
XLA Modules:
  0.0 1111.7 jit_solution(5923392795557188407)
XLA Ops:
  17.0 7.7 fusion.38
  34.2 15.1 %fusion.33 = f32[2,768,6,128]{1,2,3,0:T(8,128)S(1)} fusion(f32[2,768,6,128]{1,3,2,0:T(8,128)S(1)} %bitcast.216), kind=kOutput, calls=%fused_computation.58 | output fusion | flops 149815296 | bytes 9437184 | tf_op jit(solution)/shard_map/reduce-window.4
  52.1 4.3 broadcast_add_fusion.1
  58.9 5.2 fusion.35
  64.2 5.4 fusion.45
  72.1 46.8 %all-gather.4.cloned.1.call-done = bf16[12288,515]{1,0:T(8,128)(2,1)} async-done(((bf16[768,515]{1,0:T(8,128)(2,1)}), bf16[12288,515]{1,0:T(8,128)(2,1)}) %all-gather.4.cloned.1.call-update) | async-done | bytes 12656656 | tf_op jit(solution)/shard_map/all_gather | solution.py:13
  128.9 12.7 %fusion.61 = (bf16[12288,128]{1,0:T(8,128)(2,1)}, bf16[12288,128]{1,0:T(8,128)(2,1)}, bf16[12288,128]{1,0:T(8,128)(2,1)}, bf16[12288,128]{1,0:T(8,128)(2,1)}) fusion(bf16[12288,515]{1,0:T(8,128)(2,1)} %all-gather.4.cloned.1.call-done), kind=kLoop, calls=%fused_computation.112 | loop fusion | bytes 25165824 | tf_op jit(solution)/shard_map/slice | solution.py:15
  141.6 665.3 %while.18 = (s32[]{:T(128)}, f32[768,2,64]{0,2,1:T(8,128)}, f32[2,768]{1,0:T(2,128)S(1)}, f32[768,1,128]{0,2,1:T(8,128)}, f32[1,768]{1,0:T(1,128)S(1)}, /*index=...) while((s32[]{:T(128)}, f32[768,2,64]{0,2,1:T(8,128)}, ...), condition=%wide.region_13.14_spmd, body=%wide.region_6.13_spmd.sunk | while | flops 873221376 | bytes 114910112 | solution.py:140
  142.8 6.0 fusion.105
  148.9 15.1 %fusion.106 = f32[2,768,6,128]{1,2,3,0:T(8,128)S(1)} fusion(f32[2,768,6,128]{1,3,2,0:T(8,128)S(1)} %bitcast.214), kind=kOutput, calls=%fused_computation.2.clone.1 | output fusion | flops 149815296 | bytes 9437184 | tf_op jit(solution)/shard_map/reduce-window.12
  171.6 4.5 fusion.107
  182.6 7.5 fusion.110
  191.0 4.0 fusion.111
  198.3 6.0 fusion.105
  204.3 15.1 %fusion.106 = f32[2,768,6,128]{1,2,3,0:T(8,128)S(1)} fusion(f32[2,768,6,128]{1,3,2,0:T(8,128)S(1)} %bitcast.214), kind=kOutput, calls=%fused_computation.2.clone.1 | output fusion | flops 149815296 | bytes 9437184 | tf_op jit(solution)/shard_map/reduce-window.12
  227.0 4.5 fusion.107
  238.0 7.5 fusion.110
  246.5 4.0 fusion.111
  253.8 6.0 fusion.105
  259.8 15.1 %fusion.106 = f32[2,768,6,128]{1,2,3,0:T(8,128)S(1)} fusion(f32[2,768,6,128]{1,3,2,0:T(8,128)S(1)} %bitcast.214), kind=kOutput, calls=%fused_computation.2.clone.1 | output fusion | flops 149815296 | bytes 9437184 | tf_op jit(solution)/shard_map/reduce-window.12
  282.4 4.5 fusion.107
  293.5 7.5 fusion.110
  309.2 6.0 fusion.105
  315.2 15.1 %fusion.106 = f32[2,768,6,128]{1,2,3,0:T(8,128)S(1)} fusion(f32[2,768,6,128]{1,3,2,0:T(8,128)S(1)} %bitcast.214), kind=kOutput, calls=%fused_computation.2.clone.1 | output fusion | flops 149815296 | bytes 9437184 | tf_op jit(solution)/shard_map/reduce-window.12
  337.9 4.5 fusion.107
  348.9 7.5 fusion.110
  364.6 6.0 fusion.105
  370.6 15.1 %fusion.106 = f32[2,768,6,128]{1,2,3,0:T(8,128)S(1)} fusion(f32[2,768,6,128]{1,3,2,0:T(8,128)S(1)} %bitcast.214), kind=kOutput, calls=%fused_computation.2.clone.1 | output fusion | flops 149815296 | bytes 9437184 | tf_op jit(solution)/shard_map/reduce-window.12
  393.3 4.5 fusion.107
  404.3 7.5 fusion.110
  420.0 6.0 fusion.105
  426.0 15.1 %fusion.106 = f32[2,768,6,128]{1,2,3,0:T(8,128)S(1)} fusion(f32[2,768,6,128]{1,3,2,0:T(8,128)S(1)} %bitcast.214), kind=kOutput, calls=%fused_computation.2.clone.1 | output fusion | flops 149815296 | bytes 9437184 | tf_op jit(solution)/shard_map/reduce-window.12
  448.7 4.5 fusion.107
  459.7 7.5 fusion.110
  475.5 6.0 fusion.105
  481.5 15.1 %fusion.106 = f32[2,768,6,128]{1,2,3,0:T(8,128)S(1)} fusion(f32[2,768,6,128]{1,3,2,0:T(8,128)S(1)} %bitcast.214), kind=kOutput, calls=%fused_computation.2.clone.1 | output fusion | flops 149815296 | bytes 9437184 | tf_op jit(solution)/shard_map/reduce-window.12
  504.2 4.5 fusion.107
  515.2 7.5 fusion.110
  530.9 6.0 fusion.105
  536.9 15.1 %fusion.106 = f32[2,768,6,128]{1,2,3,0:T(8,128)S(1)} fusion(f32[2,768,6,128]{1,3,2,0:T(8,128)S(1)} %bitcast.214), kind=kOutput, calls=%fused_computation.2.clone.1 | output fusion | flops 149815296 | bytes 9437184 | tf_op jit(solution)/shard_map/reduce-window.12
  559.6 4.5 fusion.107
  570.6 7.5 fusion.110
  586.3 6.0 fusion.105
  592.3 15.1 %fusion.106 = f32[2,768,6,128]{1,2,3,0:T(8,128)S(1)} fusion(f32[2,768,6,128]{1,3,2,0:T(8,128)S(1)} %bitcast.214), kind=kOutput, calls=%fused_computation.2.clone.1 | output fusion | flops 149815296 | bytes 9437184 | tf_op jit(solution)/shard_map/reduce-window.12
  615.0 4.5 fusion.107
  626.0 7.5 fusion.110
  641.7 6.0 fusion.105
  647.7 15.1 %fusion.106 = f32[2,768,6,128]{1,2,3,0:T(8,128)S(1)} fusion(f32[2,768,6,128]{1,3,2,0:T(8,128)S(1)} %bitcast.214), kind=kOutput, calls=%fused_computation.2.clone.1 | output fusion | flops 149815296 | bytes 9437184 | tf_op jit(solution)/shard_map/reduce-window.12
  670.4 4.5 fusion.107
  681.4 7.5 fusion.110
  697.2 6.0 fusion.105
  703.2 15.1 %fusion.106 = f32[2,768,6,128]{1,2,3,0:T(8,128)S(1)} fusion(f32[2,768,6,128]{1,3,2,0:T(8,128)S(1)} %bitcast.214), kind=kOutput, calls=%fused_computation.2.clone.1 | output fusion | flops 149815296 | bytes 9437184 | tf_op jit(solution)/shard_map/reduce-window.12
  725.9 4.5 fusion.107
  736.9 7.5 fusion.110
  752.6 6.0 fusion.105
  758.6 15.1 %fusion.106 = f32[2,768,6,128]{1,2,3,0:T(8,128)S(1)} fusion(f32[2,768,6,128]{1,3,2,0:T(8,128)S(1)} %bitcast.214), kind=kOutput, calls=%fused_computation.2.clone.1 | output fusion | flops 149815296 | bytes 9437184 | tf_op jit(solution)/shard_map/reduce-window.12
  781.3 4.5 fusion.107
  792.3 7.5 fusion.110
  811.9 4.6 all-to-all-start
  816.5 38.3 %all-to-all-done = bf16[8,96,2048]{2,1,0:T(8,128)(2,1)} async-done(((bf16[8,96,2048]{2,1,0:T(8,128)(2,1)}), bf16[8,96,2048]{2,1,0:T(8,128)(2,1)}, u32[]{:S(2)}, u32[]{:S(2)}) %all-to-all-start) | async-done | bytes 3145760 | tf_op jit(solution)/shard_map/all_to_all | solution.py:28
  858.6 191.5 %all-gather.6.cloned.1.call-done = bf16[768,2048]{1,0:T(8,128)(2,1)} async-done(((bf16[96,2048]{1,0:T(8,128)(2,1)}), bf16[768,2048]{1,0:T(8,128)(2,1)}) %all-gather.6.cloned.1.call-update) | async-done | bytes 3145744 | tf_op jit(solution)/shard_map/all_gather | solution.py:153
  1050.1 5.2 fusion.43
  1055.3 11.8 %convolution_convert_fusion = bf16[768,2048]{1,0:T(8,128)(2,1)} fusion(bf16[2048,2112]{0,1:T(8,128)(2,1)} %all-gather.8.cloned.1.call-done, f32[768,704]{0,1:T(8,128)S(1)} %fusion.43, bf16[768,2048]{1,0:T(8,128)(2,1)} %all-gather.6.cloned.1.call-done), kind=kOutput, calls=%fused_computation.71 | convolution fusion | flops 4434001920 | bytes 14221312 | tf_op jit(solution)/shard_map/dot_general | solution.py:158
  1067.1 36.0 %reduce-scatter.2.cloned.1.call-done = bf16[96,2048]{1,0:T(8,128)(2,1)} async-done(((bf16[768,2048]{1,0:T(8,128)(2,1)}), bf16[96,2048]{1,0:T(8,128)(2,1)}) %reduce-scatter.2.cloned.1.call-update) | async-done | bytes 393232 | tf_op jit(solution)/shard_map/reduce_scatter | solution.py:157
  (505 shorter events, 304.3 us)
Async XLA Ops:
  6.5 801.5 %copy-start = (bf16[128,2048]{1,0:T(8,128)(2,1)S(1)}, bf16[128,2048]{1,0:T(8,128)(2,1)}, u32[]{:S(2)}) copy-start(bf16[128,2048]{1,0:T(8,128)(2,1)} %param.25) | copy-start | bytes 1572868
  6.5 6.1 copy-start.24
  6.5 7.1 copy-start.23
  6.5 6.1 copy-start.14
  6.5 6.3 copy-start.15
  6.6 7.2 copy-start.18
  6.6 5.2 copy-start.20
  6.6 5.2 copy-start.22
  6.6 5.2 copy-start.21
  6.6 7.1 copy-start.26
  6.6 112.3 %all-gather.4.cloned.1.call-start = ((), (), s32[]{:S(2)}) async-start(), calls=%async_computation.2 | async-start | bytes 16711680 | tf_op jit(solution)/shard_map/all_gather | solution.py:13
  11.7 846.9 %all-gather.8.cloned.1.call-start = ((), (), s32[]{:S(2)}) async-start(), calls=%async_computation.4 | async-start | bytes 9191424 | tf_op jit(solution)/shard_map/all_gather | solution.py:13
  17.0 10.0 copy-start.9
  30.2 4.0 copy-start.8
  30.2 4.0 copy-start.11
  34.2 15.2 %copy-start.2 = (f32[2,768,768]{1,2,0:T(8,128)}, f32[2,768,768]{1,2,0:T(8,128)S(1)}, u32[]{:S(2)}) copy-start(f32[2,768,768]{1,2,0:T(8,128)S(1)} %get-tuple-element.239) | copy-start | bytes 14155780
  34.2 23.7 %slice-start.2 = ((s8[4718592]{0:T(1024)(128)(4,1)}), s8[524288]{0:T(1024)(128)(4,1)S(1)}, s32[]{:S(2)}) async-start(s8[4718592]{0:T(1024)(128)(4,1)} %bitcast.218), calls=%async_computation.8 | async-start | bytes 1048576
  49.3 2.7 copy-start.4
  52.1 5.7 slice-start.3
  64.2 5.5 copy-start.13
  64.2 6.6 copy-start.16
  166.7 4.8 slice-start
  166.8 4.8 slice-start.1
  190.9 4.1 copy-start.5
  219.4 2.7 copy-start.1
  222.2 4.8 slice-start
  222.2 4.8 slice-start.1
  246.3 4.1 copy-start.5
  277.6 4.8 slice-start
  277.6 4.8 slice-start.1
  301.8 4.1 copy-start.5
  333.0 4.8 slice-start
  333.1 4.8 slice-start.1
  357.2 4.1 copy-start.5
  388.5 4.8 slice-start
  388.5 4.8 slice-start.1
  412.6 4.1 copy-start.5
  443.9 4.8 slice-start
  443.9 4.8 slice-start.1
  468.1 4.1 copy-start.5
  496.6 2.7 copy-start.1
  499.3 4.8 slice-start
  499.3 4.8 slice-start.1
  523.5 4.1 copy-start.5
  554.7 4.8 slice-start
  554.8 4.8 slice-start.1
  578.9 4.1 copy-start.5
  610.2 4.8 slice-start
  610.2 4.8 slice-start.1
  634.3 4.1 copy-start.5
  665.6 4.8 slice-start
  665.6 4.8 slice-start.1
  689.8 4.1 copy-start.5
  721.0 4.8 slice-start
  721.0 4.8 slice-start.1
  745.2 4.1 copy-start.5
  776.5 4.8 slice-start
  776.5 4.8 slice-start.1
  800.6 4.1 copy-start.5
  811.9 4.6 copy-start.25
  811.9 43.0 %all-to-all-start = ((bf16[8,96,2048]{2,1,0:T(8,128)(2,1)}), bf16[8,96,2048]{2,1,0:T(8,128)(2,1)}, u32[]{:S(2)}, u32[]{:S(2)}) async-start(bf16[8,96,2048]{2,1,0:T(8,128)(2,1)} %bitcast.220), calls=%async_computation | async-start | bytes 6291456 | tf_op jit(solution)/shard_map/all_to_all | solution.py:28
  816.4 40.9 %copy-start.10 = (bf16[96,2048]{1,0:T(8,128)(2,1)S(1)}, bf16[96,2048]{1,0:T(8,128)(2,1)}, u32[]{:S(2)}) copy-start(bf16[96,2048]{1,0:T(8,128)(2,1)} %param.27) | copy-start | bytes 1179652
  816.5 233.6 %all-gather.6.cloned.1.call-start = ((), (), s32[]{:S(2)}) async-start(), calls=%async_computation.3 | async-start | bytes 3538944 | tf_op jit(solution)/shard_map/all_gather | solution.py:153
  858.5 244.6 %reduce-scatter.2.cloned.1.call-start = ((), (), s32[]{:S(2)}) async-start(), calls=%async_computation.5 | async-start | bytes 3538944 | tf_op jit(solution)/shard_map/reduce_scatter | solution.py:157
  (39 other events, 73.1 us)
Sparse Core Ops, SparseCore 0:
  11.8 106.9 all-gather.3
  121.0 77.9 all-gather.7
  858.6 191.3 all-gather.5
  1067.2 35.8 reduce-scatter.1
where the time goes:
time: 1120 us; the launch traced here: 1110 us
  other arithmetic  466 us (42%)
  waiting for transfers between devices  313 us (28%)
  matrix products  192 us (17%)
  local copies, waits for them, and re-layouts  120 us (11%)
  between operations  13.8 us (1%)
    another operation x52, other arithmetic  296 us
    all_gather x1, waiting for transfers between devices, on_device(): normed_rows = lax.all_gather(normed, 'tp', axis=0, tiled=True)  191 us
    dot_general x26, matrix products, stick_terms(): jnp.einsum('thd,shd->hts', query, key_heads, preferred_element_type=jnp.f...  125 us
    convert_element_type x26, other arithmetic, stick_terms(): weights = weights.astype(jnp.bfloat16)  113 us
    all_gather x2, waiting for transfers between devices, turned_gather(): whole, at, done = (lax.all_gather(both, axis, axis=0, tiled=True), 0, [])  46.8 us
    dot_general x26, matrix products, stick_terms(): jnp.einsum('hts,shd->thd', weights, value_heads, preferred_element_type=j...  46.1 us
    another operation x13, other arithmetic, stick_terms(): suffix = lax.cumsum(log_fail, axis=2, reverse=True) - log_fail  44.6 us
    while x144, local copies, waits for them, and re-layouts  40.6 us
  transfers between devices with their start and end apart: 5, of which 4 were waited for; matrix products, arithmetic and copies ran while one was open for 64% of the time, Pallas kernels for 0%

commit v1 on v0

v1 whole, which is shorter than its diff:
```python
import functools
import math

import jax
import jax.numpy as jnp
import numpy as np
from jax import lax
from jax.experimental import pallas as pl
from jax.experimental.pallas import tpu as pltpu
from jax.sharding import PartitionSpec as P

SMALL_DIM = 64
LARGE_DIM = 128
BLOCK = 768
STRIPES = 8
STRIPE = BLOCK // STRIPES
TILE = 256
LOG2E = math.log2(math.e)
MESH = pl.DeviceIdType.MESH
VMEM_LIMIT = 60 * 1024 * 1024


def vmem():
    return pl.BlockSpec(memory_space=pltpu.VMEM)


def sp_coords():
    index = lax.axis_index("sp")
    return index // 4, index % 4


def z_neighbours():
    z, x = sp_coords()
    return {"sp": ((z + 1) % 4) * 4 + x}, {"sp": ((z + 3) % 4) * 4 + x}


def x_neighbours():
    z, x = sp_coords()
    return {"sp": z * 4 + (x + 1) % 4}, {"sp": z * 4 + (x + 3) % 4}


def y_neighbours():
    t = lax.axis_index("tp")
    return {"tp": (t + 2) % 8}, {"tp": (t + 6) % 8}


def sibling():
    t = lax.axis_index("tp")
    return {"tp": t + 1 - 2 * (t % 2)}


def greet(devices):
    barrier = pltpu.get_barrier_semaphore()
    for device in devices:
        pl.semaphore_signal(barrier, inc=1, device_id=device, device_id_type=MESH)
    pl.semaphore_wait(barrier, len(devices))


class Copies:
    def __init__(self, send_sems, recv_sems):
        self.send_sems, self.recv_sems, self.used, self.all = send_sems, recv_sems, 0, []

    def make(self, src, dst, device):
        k = self.used
        self.used += 1
        copy = pltpu.make_async_remote_copy(
            src_ref=src,
            dst_ref=dst,
            send_sem=self.send_sems.at[k],
            recv_sem=self.recv_sems.at[k],
            device_id=device,
            device_id_type=MESH,
        )
        self.all.append(copy)
        return copy

    def drain_sends(self):
        for copy in self.all:
            copy.wait_send()


def comm_call(kernel, outs, scratch, copies, collective_id, name, args):
    return pl.pallas_call(
        kernel,
        out_shape=outs,
        in_specs=[vmem()] * len(args),
        out_specs=jax.tree.map(lambda _: vmem(), outs),
        scratch_shapes=[
            *scratch,
            pltpu.SemaphoreType.DMA((copies,)),
            pltpu.SemaphoreType.DMA((copies,)),
        ],
        compiler_params=pltpu.CompilerParams(
            collective_id=collective_id, has_side_effects=True, vmem_limit_bytes=VMEM_LIMIT
        ),
        name=name,
    )(*args)


def ring_gather(copies, jobs):
    begun = []
    for own, whole, me, right, left, rows in jobs:
        to_right = copies.make(own, whole.at[me], right)
        to_left = copies.make(own, whole.at[me], left)
        to_right.start()
        to_left.start()
        begun.append((to_right, to_left))
    for own, whole, me, right, left, rows in jobs:
        whole[me] = own[...]
    later = []
    for (own, whole, me, right, left, rows), (to_right, to_left) in zip(jobs, begun):
        half = rows // 2
        before, after = (me + 3) % 4, (me + 1) % 4
        to_right.wait_recv()
        first = whole.at[before, pl.ds(0, half)]
        on_right = copies.make(first, first, right)
        on_right.start()
        to_left.wait_recv()
        second = whole.at[after, pl.ds(half, half)]
        on_left = copies.make(second, second, left)
        on_left.start()
        later.append((on_right, on_left))
    for on_right, on_left in later:
        on_right.wait_recv()
        on_left.wait_recv()
    copies.drain_sends()


def gather_kernel(q, k, v, off, q_all, k_all, v_all, off_all, send_sems, recv_sems):
    z, x = sp_coords()
    z_right, z_left = z_neighbours()
    x_right, x_left = x_neighbours()
    greet((z_right, z_left, x_right, x_left))
    ring_gather(
        Copies(send_sems, recv_sems),
        (
            (k, k_all, z, z_right, z_left, BLOCK),
            (q, q_all, x, x_right, x_left, 256),
            (v, v_all, z, z_right, z_left, 256),
            (off, off_all, z, z_right, z_left, 32),
        ),
    )


def totals_kernel(tot, tot_all, send_sems, recv_sems):
    _, x = sp_coords()
    right, left = x_neighbours()
    greet((right, left))
    ring_gather(Copies(send_sems, recv_sems), ((tot, tot_all, x, right, left, 16),))


def ring_sum(copies, parts, relay, arrived, me, right, left, rows, out):
    half = rows // 2
    top, low = pl.ds(0, half), pl.ds(half, half)
    far, after, before = (me + 2) % 4, (me + 1) % 4, (me + 3) % 4
    a = copies.make(parts.at[far, top], relay.at[0], right)
    b = copies.make(parts.at[far, low], relay.at[1], left)
    a.start()
    b.start()
    a.wait_recv()
    parts[after, top] = (
        parts[after, top].astype(jnp.float32) + relay[0].astype(jnp.float32)
    ).astype(jnp.bfloat16)
    c = copies.make(parts.at[after], arrived.at[0], right)
    c.start()
    b.wait_recv()
    parts[before, low] = (
        parts[before, low].astype(jnp.float32) + relay[1].astype(jnp.float32)
    ).astype(jnp.bfloat16)
    d = copies.make(parts.at[before], arrived.at[1], left)
    d.start()
    c.wait_recv()
    d.wait_recv()
    out[...] = (
        parts[me].astype(jnp.float32)
        + arrived[0].astype(jnp.float32)
        + arrived[1].astype(jnp.float32)
    ).astype(out.dtype)
    copies.drain_sends()


def x_sum_kernel(parts_in, out, parts, relay, arrived, send_sems, recv_sems):
    _, x = sp_coords()
    right, left = x_neighbours()
    greet((right, left))
    parts[...] = parts_in[...]
    ring_sum(Copies(send_sems, recv_sems), parts, relay, arrived, x, right, left, 256, out)


def tp_sum_kernel(terms, out, other, parts, relay, arrived, send_sems, recv_sems):
    t = lax.axis_index("tp")
    y, core = t // 2, t % 2
    right, left = y_neighbours()
    mate = sibling()
    greet((right, left, mate))
    copies = Copies(send_sems, recv_sems)
    order = [(y + step) % 4 for step in (2, 1, 3, 0)]
    given = []
    for place in order:
        copy = copies.make(terms.at[place, 1 - core], other.at[place], mate)
        copy.start()
        given.append(copy)
    for place, copy in zip(order, given):
        copy.wait_recv()
        parts[place] = (
            terms[place, core].astype(jnp.float32) + other[place].astype(jnp.float32)
        ).astype(jnp.bfloat16)
    ring_sum(copies, parts, relay, arrived, y, right, left, 96, out)


def tp_gather_kernel(own, whole, send_sems, recv_sems):
    t = lax.axis_index("tp")
    y, core = t // 2, t % 2
    right, left = y_neighbours()
    mate = sibling()
    greet((right, left, mate))
    copies = Copies(send_sems, recv_sems)
    before, after, far = (y + 3) % 4, (y + 1) % 4, (y + 2) % 4
    top, low = pl.ds(0, 48), pl.ds(48, 48)
    mine = whole.at[y, core]
    to_right = copies.make(own, mine, right)
    to_left = copies.make(own, mine, left)
    across = copies.make(own, mine, mate)
    to_right.start()
    to_left.start()
    across.start()
    whole[y, core] = own[...]
    to_right.wait_recv()
    first = whole.at[before, core, top]
    on_right = copies.make(first, first, right)
    on_right.start()
    to_left.wait_recv()
    second = whole.at[after, core, low]
    on_left = copies.make(second, second, left)
    on_left.start()
    over = [across]
    for block in (whole.at[before, core], whole.at[after, core]):
        copy = copies.make(block, block, mate)
        copy.start()
        over.append(copy)
    on_right.wait_recv()
    block = whole.at[far, core, top]
    copy = copies.make(block, block, mate)
    copy.start()
    over.append(copy)
    on_left.wait_recv()
    block = whole.at[far, core, low]
    copy = copies.make(block, block, mate)
    copy.start()
    over.append(copy)
    for copy in over:
        copy.wait_recv()
    copies.drain_sends()


def selector(head):
    rows = lax.broadcasted_iota(jnp.int32, (128, TILE), 0)
    pieces, rest = [], LOG2E
    for _ in range(3):
        piece = float(np.asarray(rest, dtype=jnp.bfloat16.dtype).astype(np.float64))
        pieces.append(piece)
        rest -= piece
    value = jnp.zeros((128, TILE), jnp.float32)
    for n, piece in enumerate(pieces):
        value = jnp.where(rows == 3 * head + n, piece, value)
    return value.astype(jnp.bfloat16)


HEADS = ((0, 0, 0, 64), (1, 0, 64, 64), (2, 128, 128, 128))


def attend_kernel(q_ref, k_ref, ext_ref, v_ref, o_ref, tot_ref, work_ref, rhs_ref):
    z, x = sp_coords()
    kb = pl.program_id(0)

    @pl.when(kb == 0)
    def _():
        tot_ref[...] = jnp.zeros_like(tot_ref)
        for head, key_column, row, rows in HEADS:
            rhs_ref[head, 128:256, :] = selector(head)
            if rows == 64:
                rhs_ref[head, 64 - row : 128 - row, :] = jnp.zeros((64, TILE), jnp.bfloat16)

    def tile(i, carry):
        place = i // 3
        first = pl.multiple_of((i % 3) * TILE, TILE)
        column = pl.multiple_of(i * TILE, TILE)
        columns = pl.ds(column, TILE)

        def run(masked):
            for head, key_column, row, rows in HEADS:
                inner = row if rows == 64 else 0
                rhs_ref[head, inner : inner + rows, :] = q_ref[place, row : row + rows, pl.ds(first, TILE)]
                rhs = rhs_ref[head]
                sums = jnp.zeros((8, TILE), jnp.float32)
                chunk = 128
                for c in reversed(range(BLOCK // chunk)):
                    span = slice(c * chunk, (c + 1) * chunk)
                    lhs = jnp.concatenate(
                        [k_ref[0, span, key_column : key_column + 128], ext_ref[0, span, :]], axis=1
                    )
                    logit = jnp.dot(lhs, rhs, preferred_element_type=jnp.float32)
                    loss = jnp.maximum(
                        logit, jnp.log2(1.0 + jnp.exp2(jnp.minimum(logit, 100.0)))
                    )
                    if masked:
                        at = lax.broadcasted_iota(jnp.int32, (chunk, TILE), 0) + c * chunk
                        key_pos = (at % 8) * STRIPE + at // 8
                        query_pos = lax.broadcasted_iota(jnp.int32, (chunk, TILE), 1) + first
                        live = key_pos < query_pos
                        loss = jnp.where(live, loss, 0.0)
                        logit = jnp.where(live, logit, -1e30)
                    for j in reversed(range(chunk // 8)):
                        eight = slice(j * 8, (j + 1) * 8)
                        sums = sums + loss[eight]
                        work_ref[c * chunk + j * 8 : c * chunk + (j + 1) * 8, :] = logit[eight] - sums
                later = [jnp.zeros((1, TILE), jnp.float32)]
                for r in range(7, 0, -1):
                    later.append(later[-1] + sums[r : r + 1])
                tot_ref[pl.ds(kb * 4 + head, 1), columns] = later[-1] + sums[0:1]
                behind = jnp.concatenate(later[::-1], axis=0)
                total = jnp.zeros((rows, TILE), jnp.float32)
                for c in range(BLOCK // 256):
                    span = slice(c * 256, (c + 1) * 256)
                    power = work_ref[span, :].reshape(32, 8, TILE) - behind[None]
                    weight = jnp.exp2(power).reshape(256, TILE).astype(jnp.bfloat16)
                    total = total + jnp.dot(
                        v_ref[0, row : row + rows, span], weight, preferred_element_type=jnp.float32
                    )
                o_ref[0, row : row + rows, columns] = total.astype(jnp.bfloat16)

        whole = jnp.logical_or(kb < z, jnp.logical_and(kb == z, place > x))
        partly = jnp.logical_and(kb == z, place == x)

        @pl.when(whole)
        def _():
            run(False)

        @pl.when(partly)
        def _():
            run(True)

        @pl.when(jnp.logical_not(jnp.logical_or(whole, partly)))
        def _():
            o_ref[0, :, columns] = jnp.zeros((256, TILE), jnp.bfloat16)

        return carry

    lax.fori_loop(0, 12, tile, 0)


def attend(q_all, k_all, ext, v_all):
    units = 12 * 8
    return pl.pallas_call(
        attend_kernel,
        grid=(4,),
        in_specs=[
            pl.BlockSpec((4, 256, BLOCK), lambda kb: (0, 0, 0)),
            pl.BlockSpec((1, BLOCK, 256), lambda kb: (kb, 0, 0)),
            pl.BlockSpec((1, BLOCK, 128), lambda kb: (kb, 0, 0)),
            pl.BlockSpec((1, 256, BLOCK), lambda kb: (kb, 0, 0)),
        ],
        out_specs=[
            pl.BlockSpec((1, 256, 4 * BLOCK), lambda kb: (kb, 0, 0)),
            pl.BlockSpec((16, 4 * BLOCK), lambda kb: (0, 0)),
        ],
        out_shape=[
            jax.ShapeDtypeStruct((4, 256, 4 * BLOCK), jnp.bfloat16),
            jax.ShapeDtypeStruct((16, 4 * BLOCK), jnp.float32),
        ],
        scratch_shapes=[
            pltpu.VMEM((BLOCK, TILE), jnp.float32),
            pltpu.VMEM((3, 256, TILE), jnp.bfloat16),
        ],
        compiler_params=pltpu.CompilerParams(
            dimension_semantics=("arbitrary",), vmem_limit_bytes=VMEM_LIMIT
        ),
        cost_estimate=pl.CostEstimate(
            flops=units * 768 * 768 * 1024, bytes_accessed=12_000_000, transcendentals=units * 768 * 768 * 9
        ),
        name="attend",
    )(q_all, k_all, ext, v_all)


def combine_kernel(o_ref, tot_ref, out_ref):
    _, x = sp_coords()
    nearer = jnp.zeros((4, TILE), jnp.float32)
    total = [None] * 3
    for kb in reversed(range(4)):
        rows = slice(kb * 4, kb * 4 + 4)
        here = jnp.zeros((4, TILE), jnp.float32)
        block = jnp.zeros((4, TILE), jnp.float32)
        for other in range(4):
            term = tot_ref[other, rows, :]
            block = block + term
            here = here + jnp.where(other > x, term, 0.0)
        factor = jnp.exp2(-(nearer + here))
        nearer = nearer + block
        for head, _, row, size in HEADS:
            term = o_ref[kb, row : row + size, :].astype(jnp.float32) * factor[head : head + 1]
            total[head] = term if total[head] is None else total[head] + term
    for head, _, row, size in HEADS:
        out_ref[0, row : row + size, :] = total[head].astype(jnp.bfloat16)


def combine(outs, totals):
    return pl.pallas_call(
        combine_kernel,
        grid=(12,),
        in_specs=[
            pl.BlockSpec((4, 256, TILE), lambda i: (0, 0, i)),
            pl.BlockSpec((4, 16, TILE), lambda i: (0, 0, i)),
        ],
        out_specs=pl.BlockSpec((1, 256, TILE), lambda i: (i // 3, 0, i % 3)),
        out_shape=jax.ShapeDtypeStruct((4, 256, BLOCK), jnp.bfloat16),
        compiler_params=pltpu.CompilerParams(dimension_semantics=("arbitrary",)),
        cost_estimate=pl.CostEstimate(
            flops=4 * 256 * 3072 * 2, bytes_accessed=9_000_000, transcendentals=50_000
        ),
        name="combine",
    )(outs, totals)


def tp_sum(terms, collective_id, name):
    shape = (96, terms.shape[-1])
    return comm_call(
        tp_sum_kernel,
        jax.ShapeDtypeStruct(shape, jnp.float32),
        [
            pltpu.VMEM((4, *shape), jnp.bfloat16),
            pltpu.VMEM((4, *shape), jnp.bfloat16),
            pltpu.VMEM((2, 48, shape[1]), jnp.bfloat16),
            pltpu.VMEM((2, *shape), jnp.bfloat16),
        ],
        8,
        collective_id,
        name,
        (terms.reshape(4, 2, *shape),),
    )


def rounded(value):
    return lax.optimization_barrier(value.astype(jnp.bfloat16)).astype(jnp.float32)


def rms_norm(stream, gain):
    scale = lax.rsqrt(jnp.mean(stream * stream, axis=-1, keepdims=True) + 1e-06)
    return (stream * scale * gain.astype(jnp.float32)).astype(jnp.bfloat16)


def striped(value):
    return value.reshape(STRIPES, STRIPE, -1).swapaxes(0, 1).reshape(BLOCK, -1)


def on_device(
    query_small, key_small, value_small, offset_small, query_large, key_large, value_large, offset_large,
    out_small, out_large, residual, norm_gain, gate_weight, up_weight, down_weight,
):
    f32, bf16 = jnp.float32, jnp.bfloat16
    scales = np.concatenate(
        [np.full(128, LOG2E * SMALL_DIM**-0.5), np.full(128, LOG2E * LARGE_DIM**-0.5)]
    ).astype(np.float32)
    query = jnp.concatenate([query_small, query_large], axis=1).astype(f32) * scales
    query = query.astype(bf16).T
    key = striped(jnp.concatenate([key_small, key_large], axis=1))
    value = striped(jnp.concatenate([value_small, value_large], axis=1)).T
    offsets = jnp.concatenate([offset_small, offset_large], axis=0)
    offsets = offsets.reshape(3, STRIPES, STRIPE).swapaxes(1, 2).reshape(3, BLOCK)
    offsets = jnp.pad(offsets, ((0, 29), (0, 0)))
    gathered = comm_call(
        gather_kernel,
        (
            jax.ShapeDtypeStruct((4, 256, BLOCK), bf16),
            jax.ShapeDtypeStruct((4, BLOCK, 256), bf16),
            jax.ShapeDtypeStruct((4, 256, BLOCK), bf16),
            jax.ShapeDtypeStruct((4, 32, BLOCK), bf16),
        ),
        [],
        16,
        0,
        "gather_qkv",
        (query, key, value, offsets),
    )
    gate_weight, up_weight, down_weight, *gathered = lax.optimization_barrier(
        (gate_weight, up_weight, down_weight, *gathered)
    )
    q_all, k_all, v_all, off_all = gathered
    weights = jnp.concatenate([gate_weight, up_weight, down_weight.T], axis=1)
    weights = lax.all_gather(weights, "sp", axis=0, tiled=True)
    width = gate_weight.shape[1]
    spread = np.zeros((32, 128), np.float32)
    for head in range(3):
        spread[head, 3 * head : 3 * head + 3] = 1
    ext = jnp.einsum(
        "bhs,hc->bsc", off_all, jnp.asarray(spread, bf16), preferred_element_type=f32
    ).astype(bf16)
    outs, totals = attend(q_all, k_all, ext, v_all)
    totals = comm_call(
        totals_kernel, jax.ShapeDtypeStruct((4, 16, 4 * BLOCK), f32), [], 4, 1, "gather_totals", (totals,)
    )
    parts = combine(outs, totals)
    mixed = comm_call(
        x_sum_kernel,
        jax.ShapeDtypeStruct((256, BLOCK), bf16),
        [
            pltpu.VMEM((4, 256, BLOCK), bf16),
            pltpu.VMEM((2, 128, BLOCK), bf16),
            pltpu.VMEM((2, 256, BLOCK), bf16),
        ],
        4,
        2,
        "sum_x",
        (parts,),
    )
    out_weight = jnp.concatenate([out_small, out_large], axis=0)
    part = lax.dot_general(mixed, out_weight, (((0,), (0,)), ((), ())), preferred_element_type=f32)
    attended = tp_sum(part.astype(bf16), 3, "sum_tp_mixed")
    stream = residual.astype(f32) + rounded(attended)
    normed = rms_norm(stream, norm_gain)
    rows = comm_call(
        tp_gather_kernel, jax.ShapeDtypeStruct((4, 2, 96, 2048), bf16), [], 9, 4, "gather_tp", (normed,)
    ).reshape(BLOCK, 2048)
    gate = jnp.dot(rows, weights[:, :width], preferred_element_type=f32)
    upper = jnp.dot(rows, weights[:, width : 2 * width], preferred_element_type=f32)
    hidden = (jax.nn.silu(gate) * upper).astype(bf16)
    down = lax.dot_general(
        hidden, weights[:, 2 * width :], (((1,), (1,)), ((), ())), preferred_element_type=f32
    )
    summed = tp_sum(down.astype(bf16), 5, "sum_tp_down")
    return (stream + rounded(summed)).astype(bf16)


def solution(mesh):
    return jax.shard_map(
        on_device,
        mesh=mesh,
        in_specs=(
            P("sp", "tp"), P("sp", "tp"), P("sp", "tp"), P("tp", "sp"),
            P("sp", "tp"), P("sp", "tp"), P("sp", "tp"), P("tp", "sp"),
            P("tp", None), P("tp", None), P(("sp", "tp"), None), P(),
            P("sp", "tp"), P("sp", "tp"), P("tp", "sp"),
        ),
        out_specs=P(("sp", "tp"), None),
        check_vma=False,
    )
```

time: 1120 us -> 276 us (0.25)
  other arithmetic: 466 us -> 8.36 us
  waiting for transfers between devices: 313 us -> 0.04 us
  Pallas kernels: 0 us -> 226 us
  matrix products: 192 us -> 22.9 us
  local copies, waits for them, and re-layouts: 120 us -> 3.47 us
    another operation x65 -> x0, other arithmetic: 341 us -> none
    all_gather x3 -> x1, waiting for transfers between devices: 238 us -> 0.02 us  [on_device(): weights = lax.all_gather(weights, 'sp', axis=0, tiled=True)]
    pallas_call x0 -> x8, Pallas kernels: none -> 226 us  [the longest x6 138 us: comm_call(): pl.pallas_call(kernel, out_shape=outs, in_specs=[vmem()] * len(args), out...]
    dot_general x56 -> x4, matrix products: 192 us -> 22.9 us  [the longest x1 11.8 us: on_device(): lax.dot_general(hidden, weights[:, 2 * width:], (((1,), (1,)), ((), ())),...]
    convert_element_type x41 -> x3, other arithmetic: 116 us -> 3.25 us  [the longest x2 2.35 us: rounded(): value.astype(jnp.bfloat16)]
    while x145 -> x0, local copies, waits for them, and re-layouts: 43.8 us -> none
    all_to_all x1 -> x0, waiting for transfers between devices: 38.3 us -> none  [summed_on_arrival(): lax.all_to_all(pieces, axis, split_axis=0, concat_axis=0, tiled=True)]
    reduce_scatter x1 -> x0, waiting for transfers between devices: 36 us -> none  [on_device(): lax.psum_scatter(jnp.dot(hidden, down_full, preferred_element_type=jnp.fl...]
  transfers between devices with their start and end apart: 5 -> 1, of which waited for: 4 -> 0; matrix products, arithmetic and copies ran while one was open for 64% -> 3% of each run, Pallas kernels for 0% -> 60%
where the time goes in v1:
time: 276 us; the launch traced here: 275 us
  Pallas kernels  226 us (82%)
  matrix products  22.9 us (8%)
  between operations  13.7 us (5%)
  other arithmetic  8.36 us (3%)
  local copies, waits for them, and re-layouts  3.47 us (1%)
    pallas_call x6, Pallas kernels, comm_call(): pl.pallas_call(kernel, out_shape=outs, in_specs=[vmem()] * len(args), out...  138 us
    pallas_call x1, Pallas kernels, attend(): pl.pallas_call(attend_kernel, grid=(4,), in_specs=[pl.BlockSpec((4, 256,...  79 us
    dot_general x1, matrix products, on_device(): lax.dot_general(hidden, weights[:, 2 * width:], (((1,), (1,)), ((), ())),...  11.8 us
    pallas_call x1, Pallas kernels, combine(): pl.pallas_call(combine_kernel, grid=(12,), in_specs=[pl.BlockSpec((4, 256...  8.96 us
  transfers between devices with their start and end apart: 1, of which 0 were waited for; matrix products, arithmetic and copies ran while one was open for 3% of the time, Pallas kernels for 60%

profile of v1, /device:TPU:96, one launch (start us, length us, event | category | flops | bytes accessed | tf_op | source)
XLA Modules:
  0.0 275.0 jit_solution(7646999293086048123)
XLA Ops:
  6.5 0.0 copy-start.12
  6.5 0.0 copy-start.3
  6.5 0.0 copy-start.4
  6.5 0.0 copy-start.11
  6.5 0.0 copy-start.10
  6.5 0.0 all-gather.2.cloned.1.call-start
  6.6 1.2 pad_maximum_fusion.2
  7.8 0.2 copy.36
  8.0 0.0 copy-start.5
  8.0 0.0 copy-start.6
  8.0 0.0 copy-start.7
  8.0 0.9 copy.32
  9.0 1.1 pad_maximum_fusion.1
  10.0 0.0 copy-start.8
  10.0 1.0 copy.37
  11.0 0.0 copy-done.3
  11.0 0.1 copy.28
  11.2 0.0 copy-done.4
  11.2 0.1 copy.29
  11.3 0.0 copy-done.11
  11.3 0.0 copy-done.10
  11.4 0.1 reshape.41
  11.4 0.1 copy.33
  11.6 0.1 reshape.42
  11.7 0.6 pad.4.off
  12.4 0.0 copy-done.12
  12.4 0.9 fusion.13.q
  13.2 34.3 %gather_qkv.1 = (bf16[4,256,768]{2,1,0:T(8,128)(2,1)}, bf16[4,768,256]{2,1,0:T(8,128)(2,1)}, bf16[4,256,768]{2,1,0:T(8,128)(2,1)}, bf16[4,32,768]{2,1,0:T(8,128)(2,1)}) custom-call(bf16[256,768]{1,0:T(8,128)(2,1)} %fusion.13.q, bf16[768,256]{1,0:T(8,128)(2,1)} %bitcast.34, bf16[256,768]{1,0:T(8,128)(2,1)} %bitcast.33, bf16[32,768]{1,0:T(8,128)(2,1)} %pad.4.off), custom_call_target="tpu_custom_call" | custom-call | tf_op jit(solution)/shard_map/gather_qkv/pallas_call | solution.py:83
  47.5 0.0 copy-done.5
  47.5 0.0 copy-done.6
  47.5 0.0 copy-done.7
  47.5 0.9 pad_maximum_fusion
  48.4 0.0 all-gather.2.cloned.1.call-update
  48.4 0.0 copy-done.8
  48.4 2.2 convolution_convert_fusion.2.ext_ref
  50.7 79.0 %attend.1 = (bf16[4,256,3072]{2,1,0:T(8,128)(2,1)}, f32[16,3072]{1,0:T(8,128)}) custom-call(bf16[4,256,768]{2,1,0:T(8,128)(2,1)} %get-tuple-element.22.q_ref, bf16[4,768,256]{2,1,0:T(8,128)(2,1)} %get-tuple-element.23.k_ref, bf16[4,768,128]{2,1,0:T(8,128)(2,1)} %convolution_convert_fusion.2.ext_ref, bf16[4,256,768]{2,1,0:T(8,128)(2,1)} %get-tuple-element.25.v_ref), custom_call_target="tpu_custom_call" | custom-call | flops 57982058496 | bytes 12000000 | tf_op jit(solution)/shard_map/attend/pallas_call | solution.py:354
  129.7 12.1 %gather_totals.1.tot_ref = f32[4,16,3072]{2,1,0:T(8,128)} custom-call(f32[16,3072]{1,0:T(8,128)} %get-tuple-element.27.tot), custom_call_target="tpu_custom_call" | custom-call | tf_op jit(solution)/shard_map/gather_totals/pallas_call | solution.py:83
  141.9 0.0 copy-start.1
  141.9 0.0 copy-start.2
  141.9 9.0 %combine.1.parts_in = bf16[4,256,768]{2,1,0:T(8,128)(2,1)} custom-call(bf16[4,256,3072]{2,1,0:T(8,128)(2,1)} %get-tuple-element.26.o_ref, f32[4,16,3072]{2,1,0:T(8,128)} %gather_totals.1.tot_ref), custom_call_target="tpu_custom_call" | custom-call | flops 6291456 | bytes 9000000 | tf_op jit(solution)/shard_map/combine/pallas_call | solution.py:407
  150.8 19.7 %sum_x.1 = bf16[256,768]{1,0:T(8,128)(2,1)} custom-call(bf16[4,256,768]{2,1,0:T(8,128)(2,1)} %combine.1.parts_in), custom_call_target="tpu_custom_call" | custom-call | tf_op jit(solution)/shard_map/sum_x/pallas_call | solution.py:83
  170.5 0.0 copy-done.1
  170.6 0.0 copy-done.2
  170.6 3.7 %convolution_convert_fusion.1 = bf16[768,2048]{1,0:T(8,128)(2,1)} fusion(bf16[256,768]{1,0:T(8,128)(2,1)} %sum_x.1, bf16[128,2048]{1,0:T(8,128)(2,1)S(1)} %copy-done.1, bf16[128,2048]{1,0:T(8,128)(2,1)S(1)} %copy-done.2), kind=kOutput, calls=%fused_computation.1 | convolution fusion | flops 808976384 | bytes 4587520 | tf_op jit(solution)/shard_map/dot_general | solution.py:516
  174.2 0.0 copy-start.9
  174.2 0.0 copy-start
  174.2 25.3 %sum_tp_mixed.1 = f32[96,2048]{1,0:T(8,128)} custom-call(bf16[4,2,96,2048]{3,2,1,0:T(8,128)(2,1)} %bitcast.26), custom_call_target="tpu_custom_call" | custom-call | tf_op jit(solution)/shard_map/sum_tp_mixed/pallas_call | solution.py:83
  199.5 1.2 convert_element_type.49
  200.7 0.0 copy-done.9
  200.7 0.0 copy-done
  200.7 0.2 multiply_reduce_fusion
  201.0 0.9 multiply_convert_fusion.1.own
  201.9 21.3 %gather_tp.1 = bf16[4,2,96,2048]{3,2,1,0:T(8,128)(2,1)} custom-call(bf16[96,2048]{1,0:T(8,128)(2,1)} %multiply_convert_fusion.1.own), custom_call_target="tpu_custom_call" | custom-call | tf_op jit(solution)/shard_map/gather_tp/pallas_call | solution.py:83
  223.1 0.0 all-gather.2.cloned.1.call-done
  223.2 5.2 %fusion.3 = f32[768,704]{0,1:T(8,128)S(1)} fusion(bf16[768,2048]{1,0:T(8,128)(2,1)} %bitcast.27, bf16[2048,2112]{0,1:T(8,128)(2,1)} %all-gather.2.cloned.1.call-done), kind=kOutput, calls=%fused_computation.5 | convolution fusion | flops 2214592512 | bytes 8192000 | tf_op jit(solution)/shard_map/dot_general | solution.py:523
  228.4 11.8 %convolution_convert_fusion = bf16[768,2048]{1,0:T(8,128)(2,1)} fusion(bf16[2048,2112]{0,1:T(8,128)(2,1)} %all-gather.2.cloned.1.call-done, f32[768,704]{0,1:T(8,128)S(1)} %fusion.3, bf16[768,2048]{1,0:T(8,128)(2,1)} %bitcast.28), kind=kOutput, calls=%fused_computation | convolution fusion | flops 4434001920 | bytes 14221312 | tf_op jit(solution)/shard_map/dot_general | solution.py:526
  240.2 25.9 %sum_tp_down.1 = f32[96,2048]{1,0:T(8,128)} custom-call(bf16[4,2,96,2048]{3,2,1,0:T(8,128)(2,1)} %bitcast.29), custom_call_target="tpu_custom_call" | custom-call | tf_op jit(solution)/shard_map/sum_tp_down/pallas_call | solution.py:83
  266.0 1.2 convert_element_type.55
  267.2 0.9 add_convert_fusion
  (3 shorter events, 0.0 us)
Async XLA Ops:
  6.5 5.8 %copy-start.12 = (f32[256]{0:T(256)S(1)}, f32[256]{0:T(256)}, u32[]{:S(2)}) copy-start(f32[256]{0:T(256)} %constant.17.clone) | copy-start | bytes 3076
  6.5 4.5 %copy-start.3 = (bf16[768,128]{1,0:T(8,128)(2,1)S(1)}, bf16[768,128]{1,0:T(8,128)(2,1)}, u32[]{:S(2)}) copy-start(bf16[768,128]{1,0:T(8,128)(2,1)} %param.17) | copy-start | bytes 589828
  6.5 4.6 %copy-start.4 = (bf16[768,128]{1,0:T(8,128)(2,1)S(1)}, bf16[768,128]{1,0:T(8,128)(2,1)}, u32[]{:S(2)}) copy-start(bf16[768,128]{1,0:T(8,128)(2,1)} %param.21) | copy-start | bytes 589828
  6.5 4.8 %copy-start.11 = (bf16[2,768]{1,0:T(2,128)(2,1)S(1)}, bf16[2,768]{1,0:T(2,128)(2,1)}, u32[]{:S(2)}) copy-start(bf16[2,768]{1,0:T(2,128)(2,1)} %param.20) | copy-start | bytes 9220
  6.5 4.8 %copy-start.10 = (bf16[1,768]{1,0:T(2,128)(2,1)S(1)}, bf16[1,768]{1,0:T(2,128)(2,1)}, u32[]{:S(2)}) copy-start(bf16[1,768]{1,0:T(2,128)(2,1)} %param.24) | copy-start | bytes 4612
  6.5 216.6 %all-gather.2.cloned.1.call-start = ((), (), s32[]{:S(2)}) async-start(), calls=%async_computation | async-start | bytes 9191424 | tf_op jit(solution)/shard_map/all_gather | solution.py:489
  8.0 39.5 %copy-start.5 = (bf16[704,128]{1,0:T(8,128)(2,1)S(1)}, bf16[704,128]{1,0:T(8,128)(2,1)}, u32[]{:S(2)}) copy-start(bf16[704,128]{1,0:T(8,128)(2,1)} %param.31) | copy-start | bytes 540676
  8.0 39.5 %copy-start.6 = (bf16[128,704]{0,1:T(8,128)(2,1)S(1)}, bf16[128,704]{0,1:T(8,128)(2,1)}, u32[]{:S(2)}) copy-start(bf16[128,704]{0,1:T(8,128)(2,1)} %param.30) | copy-start | bytes 540676
  8.0 39.5 %copy-start.7 = (bf16[128,704]{0,1:T(8,128)(2,1)S(1)}, bf16[128,704]{0,1:T(8,128)(2,1)}, u32[]{:S(2)}) copy-start(bf16[128,704]{0,1:T(8,128)(2,1)} %param.29) | copy-start | bytes 540676
  10.0 38.4 %copy-start.8 = (bf16[32,128,1]{1,0,2:T(8,128)(2,1)S(1)}, bf16[32,128,1]{1,0,2:T(8,128)(2,1)}, u32[]{:S(2)}) copy-start(bf16[32,128,1]{1,0,2:T(8,128)(2,1)} %constant.24) | copy-start | bytes 24580
  141.9 28.7 %copy-start.1 = (bf16[128,2048]{1,0:T(8,128)(2,1)S(1)}, bf16[128,2048]{1,0:T(8,128)(2,1)}, u32[]{:S(2)}) copy-start(bf16[128,2048]{1,0:T(8,128)(2,1)} %param.26) | copy-start | bytes 1572868
  141.9 28.7 %copy-start.2 = (bf16[128,2048]{1,0:T(8,128)(2,1)S(1)}, bf16[128,2048]{1,0:T(8,128)(2,1)}, u32[]{:S(2)}) copy-start(bf16[128,2048]{1,0:T(8,128)(2,1)} %param.25) | copy-start | bytes 1572868
  174.2 26.5 %copy-start.9 = (bf16[2048]{0:T(1024)(128)(2,1)S(1)}, bf16[2048]{0:T(1024)(128)(2,1)}, u32[]{:S(2)}) copy-start(bf16[2048]{0:T(1024)(128)(2,1)} %param.28) | copy-start | bytes 12292
  174.2 26.5 %copy-start = (bf16[96,2048]{1,0:T(8,128)(2,1)S(1)}, bf16[96,2048]{1,0:T(8,128)(2,1)}, u32[]{:S(2)}) copy-start(bf16[96,2048]{1,0:T(8,128)(2,1)} %param.27) | copy-start | bytes 1179652
Sparse Core Ops, SparseCore 0:
  48.5 79.3 all-gather.1

commit v2 on v1

v2 whole, which is shorter than its diff:
```python
import functools
import math

import jax
import jax.numpy as jnp
import numpy as np
from jax import lax
from jax.experimental import pallas as pl
from jax.experimental.pallas import tpu as pltpu
from jax.sharding import PartitionSpec as P

SMALL_DIM = 64
LARGE_DIM = 128
BLOCK = 768
STRIPES = 8
STRIPE = BLOCK // STRIPES
TILE = 256
HALF = BLOCK // 2
LOG2E = math.log2(math.e)
MESH = pl.DeviceIdType.MESH
VMEM_LIMIT = 60 * 1024 * 1024


def vmem():
    return pl.BlockSpec(memory_space=pltpu.VMEM)


def sp_coords():
    index = lax.axis_index("sp")
    return index // 4, index % 4


def z_neighbours():
    z, x = sp_coords()
    return {"sp": ((z + 1) % 4) * 4 + x}, {"sp": ((z + 3) % 4) * 4 + x}


def x_neighbours():
    z, x = sp_coords()
    return {"sp": z * 4 + (x + 1) % 4}, {"sp": z * 4 + (x + 3) % 4}


def mirror():
    z, x = sp_coords()
    return {"sp": (3 - z) * 4 + x}


def y_neighbours():
    t = lax.axis_index("tp")
    return {"tp": (t + 2) % 8}, {"tp": (t + 6) % 8}


def sibling():
    t = lax.axis_index("tp")
    return {"tp": t + 1 - 2 * (t % 2)}


def greet(devices):
    barrier = pltpu.get_barrier_semaphore()
    for device in devices:
        pl.semaphore_signal(barrier, inc=1, device_id=device, device_id_type=MESH)
    pl.semaphore_wait(barrier, len(devices))


class Copies:
    def __init__(self, send_sems, recv_sems):
        self.send_sems, self.recv_sems, self.used, self.all = send_sems, recv_sems, 0, []

    def make(self, src, dst, device):
        k = self.used
        self.used += 1
        copy = pltpu.make_async_remote_copy(
            src_ref=src,
            dst_ref=dst,
            send_sem=self.send_sems.at[k],
            recv_sem=self.recv_sems.at[k],
            device_id=device,
            device_id_type=MESH,
        )
        self.all.append(copy)
        return copy

    def drain_sends(self):
        for copy in self.all:
            copy.wait_send()


def comm_call(kernel, outs, scratch, copies, collective_id, name, args):
    return pl.pallas_call(
        kernel,
        out_shape=outs,
        in_specs=[vmem()] * len(args),
        out_specs=jax.tree.map(lambda _: vmem(), outs),
        scratch_shapes=[
            *scratch,
            pltpu.SemaphoreType.DMA((copies,)),
            pltpu.SemaphoreType.DMA((copies,)),
        ],
        compiler_params=pltpu.CompilerParams(
            collective_id=collective_id, has_side_effects=True, vmem_limit_bytes=VMEM_LIMIT
        ),
        name=name,
    )(*args)


def ring_gather(copies, jobs):
    begun = []
    for own, whole, me, right, left, rows, wait in jobs:
        if wait is not None:
            wait()
        half = rows // 2
        top, low = pl.ds(0, half), pl.ds(half, half)
        sent = (
            copies.make(own.at[top], whole.at[me, top], right),
            copies.make(own.at[low], whole.at[me, low], left),
            copies.make(own.at[low], whole.at[me, low], right),
            copies.make(own.at[top], whole.at[me, top], left),
        )
        for copy in sent:
            copy.start()
        whole[me] = own[...]
        begun.append(sent)
    later = []
    for (own, whole, me, right, left, rows, wait), sent in zip(jobs, begun):
        half = rows // 2
        before, after = (me + 3) % 4, (me + 1) % 4
        sent[0].wait_recv()
        first = whole.at[before, pl.ds(0, half)]
        on_right = copies.make(first, first, right)
        on_right.start()
        sent[1].wait_recv()
        second = whole.at[after, pl.ds(half, half)]
        on_left = copies.make(second, second, left)
        on_left.start()
        later += [sent[2], sent[3], on_right, on_left]
    for copy in later:
        copy.wait_recv()
    copies.drain_sends()


def gather_kernel(
    q_own, q_give, k, v, off, qa_all, qb_all, k_all, v_all, off_all, q_got, send_sems, recv_sems
):
    z, x = sp_coords()
    z_right, z_left = z_neighbours()
    x_right, x_left = x_neighbours()
    greet((z_right, z_left, x_right, x_left))
    copies = Copies(send_sems, recv_sems)
    swap = copies.make(q_give, q_got, mirror())
    swap.start()
    ring_gather(
        copies,
        (
            (k, k_all, z, z_right, z_left, BLOCK, None),
            (v, v_all, z, z_right, z_left, 256, None),
            (off, off_all, z, z_right, z_left, 32, None),
            (q_own, qa_all, x, x_right, x_left, 256, None),
            (q_got, qb_all, x, x_right, x_left, 256, swap.wait_recv),
        ),
    )


def totals_kernel(tot, tot_all, send_sems, recv_sems):
    _, x = sp_coords()
    right, left = x_neighbours()
    greet((right, left))
    ring_gather(Copies(send_sems, recv_sems), ((tot, tot_all, x, right, left, 16, None),))


def plus(a, b):
    return (a.astype(jnp.float32) + b.astype(jnp.float32)).astype(jnp.bfloat16)


class RingSum:
    def __init__(self, copies, parts, relay, arrived, me, right, left, rows):
        half = rows // 2
        self.copies, self.parts, self.relay, self.arrived = copies, parts, relay, arrived
        self.me, self.right, self.left = me, right, left
        self.top, self.low = pl.ds(0, half), pl.ds(half, half)
        self.far, self.after, self.before = (me + 2) % 4, (me + 1) % 4, (me + 3) % 4
        self.waits = []

    def send(self, src, dst, device):
        copy = self.copies.make(src, dst, device)
        copy.start()
        return copy

    def send_far(self):
        self.a = self.send(self.parts.at[self.far, self.top], self.relay.at[0], self.right)
        self.b = self.send(self.parts.at[self.far, self.low], self.relay.at[1], self.left)

    def send_after(self):
        self.waits.append(
            self.send(self.parts.at[self.after, self.low], self.arrived.at[0, self.low], self.right)
        )

    def send_before(self):
        self.waits.append(
            self.send(self.parts.at[self.before, self.top], self.arrived.at[1, self.top], self.left)
        )

    def pass_on(self):
        self.a.wait_recv()
        self.parts[self.after, self.top] = plus(self.parts[self.after, self.top], self.relay[0])
        self.waits.append(
            self.send(self.parts.at[self.after, self.top], self.arrived.at[0, self.top], self.right)
        )
        self.b.wait_recv()
        self.parts[self.before, self.low] = plus(self.parts[self.before, self.low], self.relay[1])
        self.waits.append(
            self.send(self.parts.at[self.before, self.low], self.arrived.at[1, self.low], self.left)
        )

    def finish(self, own):
        for copy in self.waits:
            copy.wait_recv()
        return own + self.arrived[0].astype(jnp.float32) + self.arrived[1].astype(jnp.float32)


def x_sum_kernel(
    parts_a, parts_b, out, pa, pb, relay_a, relay_b, arrived_a, arrived_b, give, got, send_sems, recv_sems
):
    z, x = sp_coords()
    right, left = x_neighbours()
    greet((right, left, mirror()))
    copies = Copies(send_sems, recv_sems)
    rings = []
    for source, parts, relay, arrived in (
        (parts_b, pb, relay_b, arrived_b), (parts_a, pa, relay_a, arrived_a)
    ):
        ring = RingSum(copies, parts, relay, arrived, x, right, left, 256)
        parts[...] = source[...]
        ring.send_far()
        ring.send_after()
        ring.send_before()
        rings.append(ring)
    for ring in rings:
        ring.pass_on()
    give[...] = rings[0].finish(pb[x].astype(jnp.float32)).astype(jnp.bfloat16)
    swap = copies.make(give, got, mirror())
    swap.start()
    out[0] = rings[1].finish(pa[x].astype(jnp.float32)).astype(jnp.bfloat16)
    swap.wait_recv()
    out[1] = got[...]
    copies.drain_sends()


def tp_sum_kernel(terms, out, other, parts, relay, arrived, send_sems, recv_sems):
    t = lax.axis_index("tp")
    y, core = t // 2, t % 2
    right, left = y_neighbours()
    mate = sibling()
    greet((right, left, mate))
    copies = Copies(send_sems, recv_sems)
    ring = RingSum(copies, parts, relay, arrived, y, right, left, 96)
    order = (ring.far, ring.after, ring.before, y)
    given = []
    for place in order:
        copy = copies.make(terms.at[place, 1 - core], other.at[place], mate)
        copy.start()
        given.append(copy)
    for place, copy, then in zip(order, given, (ring.send_far, ring.send_after, ring.send_before)):
        copy.wait_recv()
        parts[place] = plus(terms[place, core], other[place])
        then()
    ring.pass_on()
    given[3].wait_recv()
    own = terms[y, core].astype(jnp.float32) + other[y].astype(jnp.float32)
    out[...] = ring.finish(own)
    copies.drain_sends()


def tp_gather_kernel(own, whole, send_sems, recv_sems):
    t = lax.axis_index("tp")
    y, core = t // 2, t % 2
    right, left = y_neighbours()
    mate = sibling()
    greet((right, left, mate))
    copies = Copies(send_sems, recv_sems)
    before, after, far = (y + 3) % 4, (y + 1) % 4, (y + 2) % 4
    top, low = pl.ds(0, 48), pl.ds(48, 48)
    mine = whole.at[y, core]
    sent = (
        copies.make(own.at[top], whole.at[y, core, top], right),
        copies.make(own.at[low], whole.at[y, core, low], left),
        copies.make(own.at[low], whole.at[y, core, low], right),
        copies.make(own.at[top], whole.at[y, core, top], left),
        copies.make(own, mine, mate),
    )
    for copy in sent:
        copy.start()
    whole[y, core] = own[...]
    over = [sent[4]]

    def across(block):
        copy = copies.make(block, block, mate)
        copy.start()
        over.append(copy)

    sent[0].wait_recv()
    first = whole.at[before, core, top]
    on_right = copies.make(first, first, right)
    on_right.start()
    across(first)
    sent[1].wait_recv()
    second = whole.at[after, core, low]
    on_left = copies.make(second, second, left)
    on_left.start()
    across(second)
    sent[2].wait_recv()
    across(whole.at[before, core, low])
    sent[3].wait_recv()
    across(whole.at[after, core, top])
    on_right.wait_recv()
    across(whole.at[far, core, top])
    on_left.wait_recv()
    across(whole.at[far, core, low])
    for copy in over:
        copy.wait_recv()
    copies.drain_sends()


def selector(head):
    rows = lax.broadcasted_iota(jnp.int32, (128, TILE), 0)
    pieces, rest = [], LOG2E
    for _ in range(3):
        piece = float(np.asarray(rest, dtype=jnp.bfloat16.dtype).astype(np.float64))
        pieces.append(piece)
        rest -= piece
    value = jnp.zeros((128, TILE), jnp.float32)
    for n, piece in enumerate(pieces):
        value = jnp.where(rows == 3 * head + n, piece, value)
    return value.astype(jnp.bfloat16)


HEADS = ((0, 0, 0, 64), (1, 0, 64, 64), (2, 128, 128, 128))


def attend_kernel(qa_ref, qb_ref, k_ref, ext_ref, v_ref, o_ref, tot_ref, work_ref, rhs_ref):
    z, x = sp_coords()
    kb = pl.program_id(0)

    @pl.when(kb == 0)
    def _():
        tot_ref[...] = jnp.zeros_like(tot_ref)
        for head, key_column, row, rows in HEADS:
            rhs_ref[head, 128:256, :] = selector(head)
            if rows == 64:
                rhs_ref[head, 64 - row : 128 - row, :] = jnp.zeros((64, TILE), jnp.bfloat16)

    def tile(i, q_ref, group, own_z):
        first = pl.multiple_of(i * TILE, TILE)
        columns = pl.ds(pl.multiple_of(group * 2 * BLOCK + i * TILE, TILE), TILE)

        def run(masked):
            for head, key_column, row, rows in HEADS:
                inner = row if rows == 64 else 0
                for n in range(2):
                    piece = 2 * i + n
                    rhs_ref[head, inner : inner + rows, n * 128 : (n + 1) * 128] = q_ref[
                        piece // 3, row : row + rows, pl.ds(pl.multiple_of(piece % 3 * 128, 128), 128)
                    ]
                rhs = rhs_ref[head]
                sums = jnp.zeros((8, TILE), jnp.float32)
                chunk = 128
                if masked:
                    query = lax.broadcasted_iota(jnp.int32, (1, TILE), 1) + first
                    query_pos = query + (query // HALF - x * 2 + group) * HALF
                for c in reversed(range(BLOCK // chunk)):
                    span = slice(c * chunk, (c + 1) * chunk)
                    lhs = jnp.concatenate(
                        [k_ref[0, span, key_column : key_column + 128], ext_ref[0, span, :]], axis=1
                    )
                    logit = jnp.dot(lhs, rhs, preferred_element_type=jnp.float32)
                    loss = jnp.maximum(
                        logit, jnp.log2(1.0 + jnp.exp2(jnp.minimum(logit, 100.0)))
                    )
                    if masked:
                        at = lax.broadcasted_iota(jnp.int32, (chunk, TILE), 0) + c * chunk
                        key_pos = (at % 8) * STRIPE + at // 8
                        live = key_pos < query_pos
                        loss = jnp.where(live, loss, 0.0)
                        logit = jnp.where(live, logit, -1e30)
                    for j in reversed(range(chunk // 8)):
                        eight = slice(j * 8, (j + 1) * 8)
                        sums = sums + loss[eight]
                        work_ref[c * chunk + j * 8 : c * chunk + (j + 1) * 8, :] = logit[eight] - sums
                later = [jnp.zeros((1, TILE), jnp.float32)]
                for r in range(7, 0, -1):
                    later.append(later[-1] + sums[r : r + 1])
                tot_ref[pl.ds(kb * 4 + head, 1), columns] = later[-1] + sums[0:1]
                behind = jnp.concatenate(later[::-1], axis=0)
                total = jnp.zeros((rows, TILE), jnp.float32)
                for c in range(BLOCK // 256):
                    span = slice(c * 256, (c + 1) * 256)
                    power = work_ref[span, :].reshape(32, 8, TILE) - behind[None]
                    weight = jnp.exp2(power).reshape(256, TILE).astype(jnp.bfloat16)
                    total = total + jnp.dot(
                        v_ref[0, row : row + rows, span], weight, preferred_element_type=jnp.float32
                    )
                o_ref[0, row : row + rows, columns] = total.astype(jnp.bfloat16)

        place, last = first // HALF, (first + TILE - 1) // HALF
        whole = jnp.logical_or(kb < own_z, jnp.logical_and(kb == own_z, place > x))
        none = jnp.logical_or(kb > own_z, jnp.logical_and(kb == own_z, last < x))
        partly = jnp.logical_not(jnp.logical_or(whole, none))

        @pl.when(whole)
        def _():
            run(False)

        @pl.when(partly)
        def _():
            run(True)

        @pl.when(none)
        def _():
            o_ref[0, :, columns] = jnp.zeros((256, TILE), jnp.bfloat16)

    for group, q_ref in enumerate((qa_ref, qb_ref)):

        def body(i, carry, group=group, q_ref=q_ref):
            tile(i, q_ref, group, z if group == 0 else 3 - z)
            return carry

        lax.fori_loop(0, 6, body, 0)


def attend(qa, qb, k_all, ext, v_all):
    return pl.pallas_call(
        attend_kernel,
        grid=(4,),
        in_specs=[
            pl.BlockSpec((4, 256, HALF), lambda kb: (0, 0, 0)),
            pl.BlockSpec((4, 256, HALF), lambda kb: (0, 0, 0)),
            pl.BlockSpec((1, BLOCK, 256), lambda kb: (kb, 0, 0)),
            pl.BlockSpec((1, BLOCK, 128), lambda kb: (kb, 0, 0)),
            pl.BlockSpec((1, 256, BLOCK), lambda kb: (kb, 0, 0)),
        ],
        out_specs=[
            pl.BlockSpec((1, 256, 4 * BLOCK), lambda kb: (kb, 0, 0)),
            pl.BlockSpec((16, 4 * BLOCK), lambda kb: (0, 0)),
        ],
        out_shape=[
            jax.ShapeDtypeStruct((4, 256, 4 * BLOCK), jnp.bfloat16),
            jax.ShapeDtypeStruct((16, 4 * BLOCK), jnp.float32),
        ],
        scratch_shapes=[
            pltpu.VMEM((BLOCK, TILE), jnp.float32),
            pltpu.VMEM((3, 256, TILE), jnp.bfloat16),
        ],
        compiler_params=pltpu.CompilerParams(
            dimension_semantics=("arbitrary",), vmem_limit_bytes=VMEM_LIMIT
        ),
        cost_estimate=pl.CostEstimate(
            flops=100_000_000_000, bytes_accessed=12_000_000, transcendentals=130_000_000
        ),
        name="attend",
    )(qa, qb, k_all, ext, v_all)


def combine_kernel(oa_ref, ob_ref, ta_ref, tb_ref, outa_ref, outb_ref):
    _, x = sp_coords()
    for o_ref, tot_ref, out_ref in ((oa_ref, ta_ref, outa_ref), (ob_ref, tb_ref, outb_ref)):
        nearer = jnp.zeros((4, HALF), jnp.float32)
        factors = [None] * 4
        for kb in reversed(range(4)):
            rows = slice(kb * 4, kb * 4 + 4)
            here = jnp.zeros((4, HALF), jnp.float32)
            block = jnp.zeros((4, HALF), jnp.float32)
            for other in range(4):
                term = tot_ref[other, rows, :]
                block = block + term
                here = here + jnp.where(other > x, term, 0.0)
            factors[kb] = jnp.exp2(-(nearer + here))
            nearer = nearer + block
        for head, _, row, size in HEADS:
            total = jnp.zeros((size, HALF), jnp.float32)
            for kb in range(4):
                term = o_ref[kb, row : row + size, :].astype(jnp.float32)
                total = total + term * factors[kb][head : head + 1]
            out_ref[0, row : row + size, :] = total.astype(jnp.bfloat16)


def combine(outs, totals):
    half = jax.ShapeDtypeStruct((4, 256, HALF), jnp.bfloat16)
    return pl.pallas_call(
        combine_kernel,
        grid=(4,),
        in_specs=[
            pl.BlockSpec((4, 256, HALF), lambda i: (0, 0, i)),
            pl.BlockSpec((4, 256, HALF), lambda i: (0, 0, i + 4)),
            pl.BlockSpec((4, 16, HALF), lambda i: (0, 0, i)),
            pl.BlockSpec((4, 16, HALF), lambda i: (0, 0, i + 4)),
        ],
        out_specs=[pl.BlockSpec((1, 256, HALF), lambda i: (i, 0, 0))] * 2,
        out_shape=[half, half],
        compiler_params=pltpu.CompilerParams(dimension_semantics=("arbitrary",)),
        cost_estimate=pl.CostEstimate(
            flops=4 * 256 * 3072 * 2, bytes_accessed=9_000_000, transcendentals=50_000
        ),
        name="combine",
    )(outs, outs, totals, totals)


def tp_sum(terms, collective_id, name):
    shape = (96, terms.shape[-1])
    return comm_call(
        tp_sum_kernel,
        jax.ShapeDtypeStruct(shape, jnp.float32),
        [
            pltpu.VMEM((4, *shape), jnp.bfloat16),
            pltpu.VMEM((4, *shape), jnp.bfloat16),
            pltpu.VMEM((2, 48, shape[1]), jnp.bfloat16),
            pltpu.VMEM((2, *shape), jnp.bfloat16),
        ],
        10,
        collective_id,
        name,
        (terms.reshape(4, 2, *shape),),
    )


def rounded(value):
    return lax.optimization_barrier(value.astype(jnp.bfloat16)).astype(jnp.float32)


def rms_norm(stream, gain):
    scale = lax.rsqrt(jnp.mean(stream * stream, axis=-1, keepdims=True) + 1e-06)
    return (stream * scale * gain.astype(jnp.float32)).astype(jnp.bfloat16)


def striped(value):
    return value.reshape(STRIPES, STRIPE, -1).swapaxes(0, 1).reshape(BLOCK, -1)


def on_device(
    query_small, key_small, value_small, offset_small, query_large, key_large, value_large, offset_large,
    out_small, out_large, residual, norm_gain, gate_weight, up_weight, down_weight,
):
    f32, bf16 = jnp.float32, jnp.bfloat16
    scales = np.concatenate(
        [np.full(128, LOG2E * SMALL_DIM**-0.5), np.full(128, LOG2E * LARGE_DIM**-0.5)]
    ).astype(np.float32)
    query = jnp.concatenate([query_small, query_large], axis=1).astype(f32) * scales
    query = query.astype(bf16).T
    key = striped(jnp.concatenate([key_small, key_large], axis=1))
    value = striped(jnp.concatenate([value_small, value_large], axis=1)).T
    offsets = jnp.concatenate([offset_small, offset_large], axis=0)
    offsets = offsets.reshape(3, STRIPES, STRIPE).swapaxes(1, 2).reshape(3, BLOCK)
    offsets = jnp.pad(offsets, ((0, 29), (0, 0)))
    gathered = comm_call(
        gather_kernel,
        (
            jax.ShapeDtypeStruct((4, 256, HALF), bf16),
            jax.ShapeDtypeStruct((4, 256, HALF), bf16),
            jax.ShapeDtypeStruct((4, BLOCK, 256), bf16),
            jax.ShapeDtypeStruct((4, 256, BLOCK), bf16),
            jax.ShapeDtypeStruct((4, 32, BLOCK), bf16),
        ),
        [pltpu.VMEM((256, HALF), bf16)],
        31,
        0,
        "gather_qkv",
        (query[:, :HALF], query[:, HALF:], key, value, offsets),
    )
    gate_weight, up_weight, *gathered = lax.optimization_barrier((gate_weight, up_weight, *gathered))
    qa_all, qb_all, k_all, v_all, off_all = gathered
    width = gate_weight.shape[1]
    gate_up = jnp.concatenate([gate_weight, up_weight], axis=1)
    gate_up = lax.all_gather(gate_up, "sp", axis=0, tiled=True)
    spread = np.zeros((32, 128), np.float32)
    for head in range(3):
        spread[head, 3 * head : 3 * head + 3] = 1
    ext = jnp.einsum(
        "bhs,hc->bsc", off_all, jnp.asarray(spread, bf16), preferred_element_type=f32
    ).astype(bf16)
    outs, totals = attend(qa_all, qb_all, k_all, ext, v_all)
    totals = comm_call(
        totals_kernel, jax.ShapeDtypeStruct((4, 16, 4 * BLOCK), f32), [], 6, 1, "gather_totals", (totals,)
    )
    parts_a, parts_b = combine(outs, totals)
    buffers = [pltpu.VMEM((256, HALF), bf16)] * 2
    for shape in ((4, 256, HALF), (2, 128, HALF), (2, 256, HALF)):
        buffers = [pltpu.VMEM(shape, bf16)] * 2 + buffers
    buffers = buffers[4:6] + buffers[2:4] + buffers[0:2] + buffers[6:]
    mixed = comm_call(
        x_sum_kernel,
        jax.ShapeDtypeStruct((2, 256, HALF), bf16),
        buffers,
        13,
        2,
        "sum_x",
        (parts_a, parts_b),
    )
    mixed, down_turned = lax.optimization_barrier((mixed, down_weight.T))
    down_all = lax.all_gather(down_turned, "sp", axis=0, tiled=True)
    out_weight = jnp.concatenate([out_small, out_large], axis=0)
    part = jnp.einsum("hct,cd->htd", mixed, out_weight, preferred_element_type=f32)
    attended = tp_sum(part.astype(bf16), 3, "sum_tp_mixed")
    stream = residual.astype(f32) + rounded(attended)
    normed = rms_norm(stream, norm_gain)
    rows = comm_call(
        tp_gather_kernel, jax.ShapeDtypeStruct((4, 2, 96, 2048), bf16), [], 13, 4, "gather_tp", (normed,)
    ).reshape(BLOCK, 2048)
    gate = jnp.dot(rows, gate_up[:, :width], preferred_element_type=f32)
    upper = jnp.dot(rows, gate_up[:, width:], preferred_element_type=f32)
    hidden = (jax.nn.silu(gate) * upper).astype(bf16)
    down = lax.dot_general(hidden, down_all, (((1,), (1,)), ((), ())), preferred_element_type=f32)
    summed = tp_sum(down.astype(bf16), 5, "sum_tp_down")
    return (stream + rounded(summed)).astype(bf16)


def solution(mesh):
    return jax.shard_map(
        on_device,
        mesh=mesh,
        in_specs=(
            P("sp", "tp"), P("sp", "tp"), P("sp", "tp"), P("tp", "sp"),
            P("sp", "tp"), P("sp", "tp"), P("sp", "tp"), P("tp", "sp"),
            P("tp", None), P("tp", None), P(("sp", "tp"), None), P(),
            P("sp", "tp"), P("sp", "tp"), P("tp", "sp"),
        ),
        out_specs=P(("sp", "tp"), None),
        check_vma=False,
    )
```

time: 276 us -> 254 us (0.920)
  Pallas kernels: 226 us -> 200 us
    pallas_call x1, Pallas kernels: 79 us -> 52.8 us  [attend(): pl.pallas_call(attend_kernel, grid=(4,), in_specs=[pl.BlockSpec((4, 256,...]
    pallas_call x6, Pallas kernels: 138 us -> 142 us  [comm_call(): pl.pallas_call(kernel, out_shape=outs, in_specs=[vmem()] * len(args), out...]
    pallas_call x1, Pallas kernels: 8.96 us -> 5.21 us  [combine(): pl.pallas_call(combine_kernel, grid=(4,), in_specs=[pl.BlockSpec((4, 256,...]
  transfers between devices with their start and end apart: 1 -> 2, of which waited for: 0 -> 0; matrix products, arithmetic and copies ran while one was open for 3% -> 5% of each run, Pallas kernels for 60% -> 56%
where the time goes in v2:
time: 254 us; the launch traced here: 250 us
  Pallas kernels  200 us (79%)
  matrix products  22.9 us (9%)
  between operations  13.6 us (5%)
  other arithmetic  7.14 us (3%)
  local copies, waits for them, and re-layouts  6.15 us (2%)
    pallas_call x6, Pallas kernels, comm_call(): pl.pallas_call(kernel, out_shape=outs, in_specs=[vmem()] * len(args), out...  142 us
    pallas_call x1, Pallas kernels, attend(): pl.pallas_call(attend_kernel, grid=(4,), in_specs=[pl.BlockSpec((4, 256,...  52.8 us
    dot_general x1, matrix products, on_device(): lax.dot_general(hidden, down_all, (((1,), (1,)), ((), ())), preferred_ele...  11.8 us
    pallas_call x1, Pallas kernels, combine(): pl.pallas_call(combine_kernel, grid=(4,), in_specs=[pl.BlockSpec((4, 256,...  5.21 us
    dot_general x1, matrix products, on_device(): gate = jnp.dot(rows, gate_up[:, :width], preferred_element_type=f32)  5.21 us
  transfers between devices with their start and end apart: 2, of which 0 were waited for; matrix products, arithmetic and copies ran while one was open for 5% of the time, Pallas kernels for 56%

profile of v2, /device:TPU:96, one launch (start us, length us, event | category | flops | bytes accessed | tf_op | source)
XLA Modules:
  0.0 250.2 jit_solution(12586662066829793655)
XLA Ops:
  6.5 0.0 copy-start.4
  6.5 0.0 copy-start.3
  6.5 0.0 all-gather.3.cloned.1.call-start
  6.5 1.1 copy.30
  7.7 0.0 copy-start.9
  7.7 0.0 copy-start.10
  7.7 1.1 copy.31
  8.8 0.8 fusion.10
  9.6 0.8 fusion.13
  10.4 0.0 copy-start.5
  10.4 0.0 copy-start.6
  10.4 1.1 pad_maximum_fusion.1
  11.5 0.0 copy-start.7
  11.5 0.2 copy.40
  11.7 0.9 copy.34
  12.7 0.0 copy-done.4
  12.7 0.0 copy-done.3
  12.7 1.0 copy.41
  13.7 0.0 copy-done.9
  13.7 0.0 copy-done.10
  13.7 0.1 reshape.41
  13.8 0.1 copy.35
  13.9 0.1 reshape.42
  14.1 0.6 pad.4.off
  14.7 38.9 %gather_qkv.1 = (bf16[4,256,384]{2,1,0:T(8,128)(2,1)}, bf16[4,256,384]{2,1,0:T(8,128)(2,1)}, bf16[4,768,256]{2,1,0:T(8,128)(2,1)}, bf16[4,256,768]{2,1,0:T(8,128)(2,1)}, bf16[4,32,768]{2,1,0:T(8,128)(2,1)}) custom-call(bf16[256,384]{1,0:T(8,128)(2,1)} %get-tuple-element.42.q_own, bf16[256,384]{1,0:T(8,128)(2,1)} %get-tuple-element.41.q_give, ...), custom_call_target="tpu_custom_call" | custom-call | tf_op jit(solution)/shard_map/gather_qkv/pallas_call | solution.py:89
  53.6 0.0 copy-done.5
  53.6 0.0 copy-done.6
  53.6 0.8 pad_maximum_fusion.2
  54.4 0.0 all-gather.3.cloned.1.call-update
  54.4 0.0 all-gather.5.cloned.1.call-start
  54.5 0.0 copy-done.7
  54.5 2.2 convolution_convert_fusion.2.ext_ref
  56.7 52.8 %attend.1 = (bf16[4,256,3072]{2,1,0:T(8,128)(2,1)}, f32[16,3072]{1,0:T(8,128)}) custom-call(bf16[4,256,384]{2,1,0:T(8,128)(2,1)} %get-tuple-element.28.qa_ref, bf16[4,256,384]{2,1,0:T(8,128)(2,1)} %get-tuple-element.29.qb_ref, bf16[4,768,256]{2,1,0:T(8,128)(2,1)} %get-tuple-element.30.k_ref, bf16[4,768,128]{2,1,0:T(8,128)(2,1)} %convolution_convert_fusion.2.ext_ref, ...), custom_call_target="tpu_custom_call" | custom-call | flops 99999997952 | bytes 12000000 | tf_op jit(solution)/shard_map/attend/pallas_call | solution.py:430
  109.5 17.3 %gather_totals.1.ta_ref.tb_ref = f32[4,16,3072]{2,1,0:T(8,128)} custom-call(f32[16,3072]{1,0:T(8,128)} %get-tuple-element.34.tot), custom_call_target="tpu_custom_call" | custom-call | tf_op jit(solution)/shard_map/gather_totals/pallas_call | solution.py:89
  126.8 0.0 copy-start.1
  126.8 0.0 copy-start.2
  126.8 5.2 %combine.1 = (bf16[4,256,384]{2,1,0:T(8,128)(2,1)}, bf16[4,256,384]{2,1,0:T(8,128)(2,1)}) custom-call(bf16[4,256,3072]{2,1,0:T(8,128)(2,1)} %get-tuple-element.33.oa_ref.ob_ref, bf16[4,256,3072]{2,1,0:T(8,128)(2,1)} %get-tuple-element.33.oa_ref.ob_ref, f32[4,16,3072]{2,1,0:T(8,128)} %gather_totals.1.ta_ref.tb_ref, f32[4,16,3072]{2,1,0:T(8,128)} %gather_totals.1.ta_ref.tb_ref), custom_call_target="tpu_custom_call" | custom-call | flops 6291456 | bytes 9000000 | tf_op jit(solution)/shard_map/combine/pallas_call | solution.py:487
  132.0 22.0 %sum_x.1 = bf16[2,256,384]{2,1,0:T(8,128)(2,1)} custom-call(bf16[4,256,384]{2,1,0:T(8,128)(2,1)} %get-tuple-element.35.parts_a, bf16[4,256,384]{2,1,0:T(8,128)(2,1)} %get-tuple-element.36.parts_b), custom_call_target="tpu_custom_call" | custom-call | tf_op jit(solution)/shard_map/sum_x/pallas_call | solution.py:89
  154.0 0.0 all-gather.5.cloned.1.call-update
  154.0 0.0 copy-done.1
  154.0 0.0 copy-done.2
  154.0 3.7 %convolution_convert_fusion.1 = bf16[2,384,2048]{2,1,0:T(8,128)(2,1)} fusion(bf16[2,256,384]{2,1,0:T(8,128)(2,1)} %sum_x.1, bf16[128,2048]{1,0:T(8,128)(2,1)S(1)} %copy-done.1, bf16[128,2048]{1,0:T(8,128)(2,1)S(1)} %copy-done.2), kind=kOutput, calls=%fused_computation.1 | convolution fusion | flops 808976384 | bytes 4587520 | tf_op jit(solution)/shard_map/hct,cd->htd/dot_general | solution.py:599
  157.7 0.0 copy-start.8
  157.7 0.0 copy-start
  157.7 21.7 %sum_tp_mixed.1 = f32[96,2048]{1,0:T(8,128)} custom-call(bf16[4,2,96,2048]{3,2,1,0:T(8,128)(2,1)} %bitcast.30), custom_call_target="tpu_custom_call" | custom-call | tf_op jit(solution)/shard_map/sum_tp_mixed/pallas_call | solution.py:89
  179.5 1.2 convert_element_type.49
  180.6 0.0 copy-done.8
  180.7 0.0 copy-done
  180.7 0.2 multiply_reduce_fusion
  180.9 0.9 multiply_convert_fusion.1.own
  181.8 20.8 %gather_tp.1 = bf16[4,2,96,2048]{3,2,1,0:T(8,128)(2,1)} custom-call(bf16[96,2048]{1,0:T(8,128)(2,1)} %multiply_convert_fusion.1.own), custom_call_target="tpu_custom_call" | custom-call | tf_op jit(solution)/shard_map/gather_tp/pallas_call | solution.py:89
  202.6 0.0 all-gather.3.cloned.1.call-done
  202.6 5.2 %fusion.2 = f32[768,704]{0,1:T(8,128)S(1)} fusion(bf16[768,2048]{1,0:T(8,128)(2,1)} %bitcast.31, bf16[2048,1408]{0,1:T(8,128)(2,1)} %all-gather.3.cloned.1.call-done), kind=kOutput, calls=%fused_computation.4 | convolution fusion | flops 2214592512 | bytes 8192000 | tf_op jit(solution)/shard_map/dot_general | solution.py:606
  207.8 0.0 all-gather.5.cloned.1.call-done
  207.9 11.8 %convolution_convert_fusion = bf16[768,2048]{1,0:T(8,128)(2,1)} fusion(bf16[2048,704]{0,1:T(8,128)(2,1)} %all-gather.5.cloned.1.call-done, f32[768,704]{0,1:T(8,128)S(1)} %fusion.2, bf16[768,2048]{1,0:T(8,128)(2,1)} %bitcast.32, bf16[2048,1408]{0,1:T(8,128)(2,1)} %all-gather.3.cloned.1.call-done), kind=kOutput, calls=%fused_computation | convolution fusion | flops 4434001920 | bytes 14221312 | tf_op jit(solution)/shard_map/dot_general | solution.py:609
  219.7 21.6 %sum_tp_down.1 = f32[96,2048]{1,0:T(8,128)} custom-call(bf16[4,2,96,2048]{3,2,1,0:T(8,128)(2,1)} %bitcast.33), custom_call_target="tpu_custom_call" | custom-call | tf_op jit(solution)/shard_map/sum_tp_down/pallas_call | solution.py:89
  241.3 1.2 convert_element_type.55
  242.5 0.9 add_convert_fusion
  (4 shorter events, 0.1 us)
Async XLA Ops:
  6.5 6.1 %copy-start.4 = (bf16[768,128]{1,0:T(8,128)(2,1)S(1)}, bf16[768,128]{1,0:T(8,128)(2,1)}, u32[]{:S(2)}) copy-start(bf16[768,128]{1,0:T(8,128)(2,1)} %param.18) | copy-start | bytes 589828
  6.5 6.1 %copy-start.3 = (bf16[768,128]{1,0:T(8,128)(2,1)S(1)}, bf16[768,128]{1,0:T(8,128)(2,1)}, u32[]{:S(2)}) copy-start(bf16[768,128]{1,0:T(8,128)(2,1)} %param.22) | copy-start | bytes 589828
  6.5 196.1 %all-gather.3.cloned.1.call-start = ((), (), s32[]{:S(2)}) async-start(), calls=%async_computation | async-start | bytes 6127616 | tf_op jit(solution)/shard_map/all_gather | solution.py:571
  7.7 6.0 %copy-start.9 = (bf16[1,768]{1,0:T(2,128)(2,1)S(1)}, bf16[1,768]{1,0:T(2,128)(2,1)}, u32[]{:S(2)}) copy-start(bf16[1,768]{1,0:T(2,128)(2,1)} %param.24) | copy-start | bytes 4612
  7.7 6.0 %copy-start.10 = (bf16[2,768]{1,0:T(2,128)(2,1)S(1)}, bf16[2,768]{1,0:T(2,128)(2,1)}, u32[]{:S(2)}) copy-start(bf16[2,768]{1,0:T(2,128)(2,1)} %param.20) | copy-start | bytes 9220
  10.4 43.2 %copy-start.5 = (bf16[128,704]{0,1:T(8,128)(2,1)S(1)}, bf16[128,704]{0,1:T(8,128)(2,1)}, u32[]{:S(2)}) copy-start(bf16[128,704]{0,1:T(8,128)(2,1)} %param.30) | copy-start | bytes 540676
  10.4 43.2 %copy-start.6 = (bf16[128,704]{0,1:T(8,128)(2,1)S(1)}, bf16[128,704]{0,1:T(8,128)(2,1)}, u32[]{:S(2)}) copy-start(bf16[128,704]{0,1:T(8,128)(2,1)} %param.29) | copy-start | bytes 540676
  11.5 43.0 %copy-start.7 = (bf16[32,128,1]{1,0,2:T(8,128)(2,1)S(1)}, bf16[32,128,1]{1,0,2:T(8,128)(2,1)}, u32[]{:S(2)}) copy-start(bf16[32,128,1]{1,0,2:T(8,128)(2,1)} %constant.24) | copy-start | bytes 24580
  54.4 153.5 %all-gather.5.cloned.1.call-start = ((), (), s32[]{:S(2)}) async-start(), calls=%async_computation.1 | async-start | bytes 3063808 | tf_op jit(solution)/shard_map/all_gather | solution.py:597
  126.8 27.3 %copy-start.1 = (bf16[128,2048]{1,0:T(8,128)(2,1)S(1)}, bf16[128,2048]{1,0:T(8,128)(2,1)}, u32[]{:S(2)}) copy-start(bf16[128,2048]{1,0:T(8,128)(2,1)} %param.26) | copy-start | bytes 1572868
  126.8 27.3 %copy-start.2 = (bf16[128,2048]{1,0:T(8,128)(2,1)S(1)}, bf16[128,2048]{1,0:T(8,128)(2,1)}, u32[]{:S(2)}) copy-start(bf16[128,2048]{1,0:T(8,128)(2,1)} %param.25) | copy-start | bytes 1572868
  157.7 22.9 %copy-start.8 = (bf16[2048]{0:T(1024)(128)(2,1)S(1)}, bf16[2048]{0:T(1024)(128)(2,1)}, u32[]{:S(2)}) copy-start(bf16[2048]{0:T(1024)(128)(2,1)} %param.28) | copy-start | bytes 12292
  157.7 23.0 %copy-start = (bf16[96,2048]{1,0:T(8,128)(2,1)S(1)}, bf16[96,2048]{1,0:T(8,128)(2,1)}, u32[]{:S(2)}) copy-start(bf16[96,2048]{1,0:T(8,128)(2,1)} %param.27) | copy-start | bytes 1179652
Sparse Core Ops, SparseCore 0:
  54.5 71.5 all-gather.2
  154.1 49.9 all-gather.4

commit v3 on v2

--- a/solution.py
+++ b/solution.py
@@ -85,12 +85,16 @@
             copy.wait_send()
 
 
+def hbm():
+    return pl.BlockSpec(memory_space=pl.ANY)
+
+
 def comm_call(kernel, outs, scratch, copies, collective_id, name, args):
     return pl.pallas_call(
         kernel,
-        out_shape=outs,
-        in_specs=[vmem()] * len(args),
-        out_specs=jax.tree.map(lambda _: vmem(), outs),
+        out_shape=[jax.ShapeDtypeStruct(shape, dtype) for shape, dtype, _ in outs],
+        in_specs=[spec for _, spec in args],
+        out_specs=[spec for _, _, spec in outs],
         scratch_shapes=[
             *scratch,
             pltpu.SemaphoreType.DMA((copies,)),
@@ -100,71 +104,120 @@
             collective_id=collective_id, has_side_effects=True, vmem_limit_bytes=VMEM_LIMIT
         ),
         name=name,
-    )(*args)
-
-
-def ring_gather(copies, jobs):
-    begun = []
-    for own, whole, me, right, left, rows, wait in jobs:
-        if wait is not None:
-            wait()
-        half = rows // 2
-        top, low = pl.ds(0, half), pl.ds(half, half)
-        sent = (
-            copies.make(own.at[top], whole.at[me, top], right),
-            copies.make(own.at[low], whole.at[me, low], left),
-            copies.make(own.at[low], whole.at[me, low], right),
-            copies.make(own.at[top], whole.at[me, top], left),
-        )
-        for copy in sent:
+    )(*(array for array, _ in args))
+
+
+def by_rows(ref, part):
+    half = ref.shape[-2] // 2
+    return ref.at[(slice(None),) * (len(ref.shape) - 2) + (pl.ds(part * half, half),)]
+
+
+def by_units(ref, part):
+    half = ref.shape[0] // 2
+    return ref.at[pl.ds(part * half, half)]
+
+
+class RingGather:
+    def __init__(self, copies, own, whole, me, ring, cut=by_rows):
+        self.copies, self.own, self.whole, self.me, self.ring, self.cut = copies, own, whole, me, ring, cut
+
+    def slot(self, place, part):
+        return self.cut(self.whole.at[place], part)
+
+    def start(self):
+        right, left = self.ring
+        self.sent = []
+        for part, device in ((0, right), (1, left), (1, right), (0, left)):
+            copy = self.copies.make(self.cut(self.own, part), self.slot(self.me, part), device)
             copy.start()
-        whole[me] = own[...]
-        begun.append(sent)
-    later = []
-    for (own, whole, me, right, left, rows, wait), sent in zip(jobs, begun):
-        half = rows // 2
-        before, after = (me + 3) % 4, (me + 1) % 4
-        sent[0].wait_recv()
-        first = whole.at[before, pl.ds(0, half)]
-        on_right = copies.make(first, first, right)
-        on_right.start()
-        sent[1].wait_recv()
-        second = whole.at[after, pl.ds(half, half)]
-        on_left = copies.make(second, second, left)
-        on_left.start()
-        later += [sent[2], sent[3], on_right, on_left]
-    for copy in later:
-        copy.wait_recv()
-    copies.drain_sends()
+            self.sent.append(copy)
+
+    def pass_on(self):
+        right, left = self.ring
+        for n, (place, device) in enumerate((((self.me + 3) % 4, right), ((self.me + 1) % 4, left))):
+            self.sent[n].wait_recv()
+            block = self.slot(place, n)
+            copy = self.copies.make(block, block, device)
+            copy.start()
+            self.sent.append(copy)
+
+    def finish(self):
+        for copy in self.sent[2:]:
+            copy.wait_recv()
+
+
+class Keep:
+    def __init__(self, sems):
+        self.sems, self.all = sems, []
+
+    def start(self, src, dst):
+        copy = pltpu.make_async_copy(src, dst, self.sems.at[len(self.all)])
+        copy.start()
+        self.all.append(copy)
+
+    def finish(self):
+        for copy in self.all:
+            copy.wait()
 
 
 def gather_kernel(
-    q_own, q_give, k, v, off, qa_all, qb_all, k_all, v_all, off_all, q_got, send_sems, recv_sems
+    q_own, q_give, k, v, off, gate, down, qa_all, qb_all, k_all, v_all, off_all, g1, d1, q_got, keep_sems,
+    send_sems, recv_sems,
 ):
     z, x = sp_coords()
-    z_right, z_left = z_neighbours()
-    x_right, x_left = x_neighbours()
-    greet((z_right, z_left, x_right, x_left))
-    copies = Copies(send_sems, recv_sems)
+    zs, xs = z_neighbours(), x_neighbours()
+    greet((*zs, *xs))
+    copies, keep = Copies(send_sems, recv_sems), Keep(keep_sems)
     swap = copies.make(q_give, q_got, mirror())
     swap.start()
-    ring_gather(
-        copies,
-        (
-            (k, k_all, z, z_right, z_left, BLOCK, None),
-            (v, v_all, z, z_right, z_left, 256, None),
-            (off, off_all, z, z_right, z_left, 32, None),
-            (q_own, qa_all, x, x_right, x_left, 256, None),
-            (q_got, qb_all, x, x_right, x_left, 256, swap.wait_recv),
-        ),
-    )
-
-
-def totals_kernel(tot, tot_all, send_sems, recv_sems):
-    _, x = sp_coords()
-    right, left = x_neighbours()
-    greet((right, left))
-    ring_gather(Copies(send_sems, recv_sems), ((tot, tot_all, x, right, left, 16, None),))
+    first = down.at[pl.ds(0, down.shape[0] // 2)]
+    jobs = [
+        RingGather(copies, k, k_all, z, zs),
+        RingGather(copies, v, v_all, z, zs),
+        RingGather(copies, off, off_all, z, zs),
+        RingGather(copies, q_own, qa_all, x, xs),
+        RingGather(copies, q_got, qb_all, x, xs),
+        RingGather(copies, gate, g1, x, xs),
+        RingGather(copies, first, d1, x, xs),
+    ]
+    for n, job in enumerate(jobs):
+        if n == 4:
+            swap.wait_recv()
+        job.start()
+    keep.start(gate, g1.at[x])
+    keep.start(first, d1.at[x])
+    for own, whole, me in ((k, k_all, z), (v, v_all, z), (off, off_all, z), (q_own, qa_all, x), (q_got, qb_all, x)):
+        whole[me] = own[...]
+    for job in jobs:
+        job.pass_on()
+    for job in jobs:
+        job.finish()
+    keep.finish()
+    copies.drain_sends()
+
+
+def totals_kernel(tot, up, down, tot_all, u1, d2, keep_sems, send_sems, recv_sems):
+    z, x = sp_coords()
+    zs, xs = z_neighbours(), x_neighbours()
+    greet((*zs, *xs))
+    copies, keep = Copies(send_sems, recv_sems), Keep(keep_sems)
+    second = down.at[pl.ds(down.shape[0] // 2, down.shape[0] // 2)]
+    jobs = [
+        RingGather(copies, tot, tot_all, x, xs),
+        RingGather(copies, up, u1, z, zs),
+        RingGather(copies, second, d2, z, zs),
+    ]
+    for job in jobs:
+        job.start()
+    keep.start(up, u1.at[z])
+    keep.start(second, d2.at[z])
+    tot_all[x] = tot[...]
+    for job in jobs:
+        job.pass_on()
+    for job in jobs:
+        job.finish()
+    keep.finish()
+    copies.drain_sends()
 
 
 def plus(a, b):
@@ -218,12 +271,15 @@
 
 
 def x_sum_kernel(
-    parts_a, parts_b, out, pa, pb, relay_a, relay_b, arrived_a, arrived_b, give, got, send_sems, recv_sems
+    parts_a, parts_b, d1, out, dd1, pa, pb, relay_a, relay_b, arrived_a, arrived_b, give, got, send_sems, recv_sems
 ):
     z, x = sp_coords()
     right, left = x_neighbours()
-    greet((right, left, mirror()))
+    zs = z_neighbours()
+    greet((right, left, *zs))
     copies = Copies(send_sems, recv_sems)
+    weights = RingGather(copies, d1, dd1, z, zs, by_units)
+    weights.start()
     rings = []
     for source, parts, relay, arrived in (
         (parts_b, pb, relay_b, arrived_b), (parts_a, pa, relay_a, arrived_a)
@@ -236,22 +292,37 @@
         rings.append(ring)
     for ring in rings:
         ring.pass_on()
+    weights.pass_on()
     give[...] = rings[0].finish(pb[x].astype(jnp.float32)).astype(jnp.bfloat16)
     swap = copies.make(give, got, mirror())
     swap.start()
     out[0] = rings[1].finish(pa[x].astype(jnp.float32)).astype(jnp.bfloat16)
     swap.wait_recv()
     out[1] = got[...]
+    weights.finish()
     copies.drain_sends()
 
 
-def tp_sum_kernel(terms, out, other, parts, relay, arrived, send_sems, recv_sems):
+def tp_sum_kernel(with_weights, *refs):
+    if with_weights:
+        terms, d2, g1, u1, out, dd2, ga, ua, other, parts, relay, arrived, send_sems, recv_sems = refs
+    else:
+        terms, out, other, parts, relay, arrived, send_sems, recv_sems = refs
     t = lax.axis_index("tp")
     y, core = t // 2, t % 2
     right, left = y_neighbours()
     mate = sibling()
-    greet((right, left, mate))
+    z, x = sp_coords()
+    zs, xs = z_neighbours(), x_neighbours()
+    greet((right, left, mate, *zs, *xs) if with_weights else (right, left, mate))
     copies = Copies(send_sems, recv_sems)
+    weights = []
+    if with_weights:
+        weights = [
+            RingGather(copies, d2, dd2, x, xs, by_units),
+            RingGather(copies, g1.at[pl.ds(0, 2)], ga, z, zs, by_units),
+            RingGather(copies, u1.at[pl.ds(0, 1)], ua, x, xs),
+        ]
     ring = RingSum(copies, parts, relay, arrived, y, right, left, 96)
     order = (ring.far, ring.after, ring.before, y)
     given = []
@@ -259,24 +330,36 @@
         copy = copies.make(terms.at[place, 1 - core], other.at[place], mate)
         copy.start()
         given.append(copy)
+    for job in weights:
+        job.start()
     for place, copy, then in zip(order, given, (ring.send_far, ring.send_after, ring.send_before)):
         copy.wait_recv()
         parts[place] = plus(terms[place, core], other[place])
         then()
     ring.pass_on()
+    for job in weights:
+        job.pass_on()
     given[3].wait_recv()
     own = terms[y, core].astype(jnp.float32) + other[y].astype(jnp.float32)
     out[...] = ring.finish(own)
+    for job in weights:
+        job.finish()
     copies.drain_sends()
 
 
-def tp_gather_kernel(own, whole, send_sems, recv_sems):
+def tp_gather_kernel(own, g1, u1, whole, gb, ub, send_sems, recv_sems):
     t = lax.axis_index("tp")
     y, core = t // 2, t % 2
     right, left = y_neighbours()
     mate = sibling()
-    greet((right, left, mate))
+    z, x = sp_coords()
+    zs, xs = z_neighbours(), x_neighbours()
+    greet((right, left, mate, *zs, *xs))
     copies = Copies(send_sems, recv_sems)
+    weights = [
+        RingGather(copies, g1.at[pl.ds(2, 2)], gb, z, zs, by_units),
+        RingGather(copies, u1.at[pl.ds(1, 3)], ub, x, xs),
+    ]
     before, after, far = (y + 3) % 4, (y + 1) % 4, (y + 2) % 4
     top, low = pl.ds(0, 48), pl.ds(48, 48)
     mine = whole.at[y, core]
@@ -289,6 +372,8 @@
     )
     for copy in sent:
         copy.start()
+    for job in weights:
+        job.start()
     whole[y, core] = own[...]
     over = [sent[4]]
 
@@ -311,12 +396,16 @@
     across(whole.at[before, core, low])
     sent[3].wait_recv()
     across(whole.at[after, core, top])
+    for job in weights:
+        job.pass_on()
     on_right.wait_recv()
     across(whole.at[far, core, top])
     on_left.wait_recv()
     across(whole.at[far, core, low])
     for copy in over:
         copy.wait_recv()
+    for job in weights:
+        job.finish()
     copies.drain_sends()
 
 
@@ -503,22 +592,120 @@
     )(outs, outs, totals, totals)
 
 
-def tp_sum(terms, collective_id, name):
+def tp_sum(terms, collective_id, name, weights=()):
     shape = (96, terms.shape[-1])
-    return comm_call(
-        tp_sum_kernel,
-        jax.ShapeDtypeStruct(shape, jnp.float32),
+    bf16 = jnp.bfloat16
+    outs, args = [(shape, jnp.float32, vmem())], [(terms.reshape(4, 2, *shape), vmem())]
+    if weights:
+        d2, g1, u1 = weights
+        args += [(array, hbm()) for array in weights]
+        outs += [
+            ((4, *d2.shape), bf16, hbm()),
+            ((4, 2, *g1.shape[1:]), bf16, hbm()),
+            ((4, 1, *u1.shape[1:]), bf16, hbm()),
+        ]
+    out = comm_call(
+        functools.partial(tp_sum_kernel, bool(weights)),
+        outs,
         [
-            pltpu.VMEM((4, *shape), jnp.bfloat16),
-            pltpu.VMEM((4, *shape), jnp.bfloat16),
-            pltpu.VMEM((2, 48, shape[1]), jnp.bfloat16),
-            pltpu.VMEM((2, *shape), jnp.bfloat16),
-        ],
-        10,
+            pltpu.VMEM((4, *shape), bf16),
+            pltpu.VMEM((4, *shape), bf16),
+            pltpu.VMEM((2, 48, shape[1]), bf16),
+            pltpu.VMEM((2, *shape), bf16),
+        ],
+        28 if weights else 10,
         collective_id,
         name,
-        (terms.reshape(4, 2, *shape),),
+        args,
     )
+    return out if weights else out[0]
+
+
+def feed_kernel(
+    rows, g1, ga, gb, u1, ua, ub, d1, dd1, d2, dd2, out, r_vmem, gate_w, up_w, down_w, gate, hidden, sems
+):
+    z, x = sp_coords()
+    half = d1.shape[1]
+    row_copy = pltpu.make_async_copy(rows, r_vmem, sems.at[64])
+    row_copy.start()
+    waits = [[], [], []]
+
+    def fetch(stage, mine, own, other, dst, n):
+        kept = pltpu.make_async_copy(own, dst, sems.at[n])
+        came = pltpu.make_async_copy(other, dst, sems.at[n])
+        pl.when(mine)(kept.start)
+        pl.when(jnp.logical_not(mine))(came.start)
+        waits[stage].append(came)
+
+    spots = [(zp, xp, pl.ds((zp * 4 + xp) * 128, 128)) for zp in range(4) for xp in range(4)]
+    for n, (zp, xp, lanes) in enumerate(spots):
+        fetch(0, z == zp, g1.at[xp], (ga, gb)[xp // 2].at[zp, xp % 2], gate_w.at[:, lanes], n)
+    for n, (zp, xp, lanes) in enumerate(spots):
+        other = ua.at[xp, 0] if zp == 0 else ub.at[xp, zp - 1]
+        fetch(1, x == xp, u1.at[zp], other, up_w.at[:, lanes], 16 + n)
+    for n, (zp, xp, lanes) in enumerate(spots):
+        fetch(2, z == zp, d1.at[xp], dd1.at[zp, xp], down_w.at[pl.ds(0, half), lanes], 32 + n)
+        fetch(2, x == xp, d2.at[zp], dd2.at[xp, zp], down_w.at[pl.ds(half, half), lanes], 48 + n)
+    turned = (((1,), (1,)), ((), ()))
+
+    def over_rows(step):
+        lax.fori_loop(0, 3, lambda i, c: (step(pl.ds(pl.multiple_of(i * 256, 256), 256)), c)[1], 0)
+
+    row_copy.wait()
+    for copy in waits[0]:
+        copy.wait()
+
+    def gates(span):
+        gate[span, :] = lax.dot_general(
+            r_vmem[span, :], gate_w[...], turned, preferred_element_type=jnp.float32
+        )
+
+    over_rows(gates)
+    for copy in waits[1]:
+        copy.wait()
+
+    def hide(span):
+        upper = lax.dot_general(
+            r_vmem[span, :], up_w[...], turned, preferred_element_type=jnp.float32
+        )
+        value = gate[span, :]
+        hidden[span, :] = (value / (1.0 + jnp.exp(-value)) * upper).astype(jnp.bfloat16)
+
+    over_rows(hide)
+    for copy in waits[2]:
+        copy.wait()
+
+    def lower(span):
+        out[span, :] = jnp.dot(
+            hidden[span, :], down_w[...], preferred_element_type=jnp.float32
+        ).astype(jnp.bfloat16)
+
+    over_rows(lower)
+
+
+def feed(rows, *weights):
+    units = weights[0].shape[1]
+    bf16 = jnp.bfloat16
+    return pl.pallas_call(
+        feed_kernel,
+        out_shape=jax.ShapeDtypeStruct((BLOCK, 2048), bf16),
+        in_specs=[hbm()] * (1 + len(weights)),
+        out_specs=vmem(),
+        scratch_shapes=[
+            pltpu.VMEM((BLOCK, 2048), bf16),
+            pltpu.VMEM((units, 2048), bf16),
+            pltpu.VMEM((units, 2048), bf16),
+            pltpu.VMEM((units, 2048), bf16),
+            pltpu.VMEM((BLOCK, units), jnp.float32),
+            pltpu.VMEM((BLOCK, units), bf16),
+            pltpu.SemaphoreType.DMA((65,)),
+        ],
+        compiler_params=pltpu.CompilerParams(vmem_limit_bytes=VMEM_LIMIT),
+        cost_estimate=pl.CostEstimate(
+            flops=6 * BLOCK * 2048 * units, bytes_accessed=15_000_000, transcendentals=BLOCK * units
+        ),
+        name="feed",
+    )(rows, *weights)
 
 
 def rounded(value):
@@ -549,26 +736,25 @@
     offsets = jnp.concatenate([offset_small, offset_large], axis=0)
     offsets = offsets.reshape(3, STRIPES, STRIPE).swapaxes(1, 2).reshape(3, BLOCK)
     offsets = jnp.pad(offsets, ((0, 29), (0, 0)))
-    gathered = comm_call(
+    gate, up, down = gate_weight.T, up_weight.T, down_weight
+    units = down.shape[0]
+    qa_all, qb_all, k_all, v_all, off_all, g1, d1 = comm_call(
         gather_kernel,
-        (
-            jax.ShapeDtypeStruct((4, 256, HALF), bf16),
-            jax.ShapeDtypeStruct((4, 256, HALF), bf16),
-            jax.ShapeDtypeStruct((4, BLOCK, 256), bf16),
-            jax.ShapeDtypeStruct((4, 256, BLOCK), bf16),
-            jax.ShapeDtypeStruct((4, 32, BLOCK), bf16),
-        ),
-        [pltpu.VMEM((256, HALF), bf16)],
-        31,
+        [
+            ((4, 256, HALF), bf16, vmem()),
+            ((4, 256, HALF), bf16, vmem()),
+            ((4, BLOCK, 256), bf16, vmem()),
+            ((4, 256, BLOCK), bf16, vmem()),
+            ((4, 32, BLOCK), bf16, vmem()),
+            ((4, units, 128), bf16, hbm()),
+            ((4, units // 2, 128), bf16, hbm()),
+        ],
+        [pltpu.VMEM((256, HALF), bf16), pltpu.SemaphoreType.DMA((2,))],
+        43,
         0,
         "gather_qkv",
-        (query[:, :HALF], query[:, HALF:], key, value, offsets),
+        [(array, vmem()) for array in (query[:, :HALF], query[:, HALF:], key, value, offsets, gate, down)],
     )
-    gate_weight, up_weight, *gathered = lax.optimization_barrier((gate_weight, up_weight, *gathered))
-    qa_all, qb_all, k_all, v_all, off_all = gathered
-    width = gate_weight.shape[1]
-    gate_up = jnp.concatenate([gate_weight, up_weight], axis=1)
-    gate_up = lax.all_gather(gate_up, "sp", axis=0, tiled=True)
     spread = np.zeros((32, 128), np.float32)
     for head in range(3):
         spread[head, 3 * head : 3 * head + 3] = 1
@@ -576,38 +762,53 @@
         "bhs,hc->bsc", off_all, jnp.asarray(spread, bf16), preferred_element_type=f32
     ).astype(bf16)
     outs, totals = attend(qa_all, qb_all, k_all, ext, v_all)
-    totals = comm_call(
-        totals_kernel, jax.ShapeDtypeStruct((4, 16, 4 * BLOCK), f32), [], 6, 1, "gather_totals", (totals,)
+    totals, u1, d2 = comm_call(
+        totals_kernel,
+        [
+            ((4, 16, 4 * BLOCK), f32, vmem()),
+            ((4, units, 128), bf16, hbm()),
+            ((4, units // 2, 128), bf16, hbm()),
+        ],
+        [pltpu.SemaphoreType.DMA((2,))],
+        18,
+        1,
+        "gather_totals",
+        [(array, vmem()) for array in (totals, up, down)],
     )
     parts_a, parts_b = combine(outs, totals)
     buffers = [pltpu.VMEM((256, HALF), bf16)] * 2
     for shape in ((4, 256, HALF), (2, 128, HALF), (2, 256, HALF)):
         buffers = [pltpu.VMEM(shape, bf16)] * 2 + buffers
     buffers = buffers[4:6] + buffers[2:4] + buffers[0:2] + buffers[6:]
-    mixed = comm_call(
+    mixed, dd1 = comm_call(
         x_sum_kernel,
-        jax.ShapeDtypeStruct((2, 256, HALF), bf16),
+        [((2, 256, HALF), bf16, vmem()), ((4, *d1.shape), bf16, hbm())],
         buffers,
-        13,
+        19,
         2,
         "sum_x",
-        (parts_a, parts_b),
+        [(parts_a, vmem()), (parts_b, vmem()), (d1, hbm())],
     )
-    mixed, down_turned = lax.optimization_barrier((mixed, down_weight.T))
-    down_all = lax.all_gather(down_turned, "sp", axis=0, tiled=True)
     out_weight = jnp.concatenate([out_small, out_large], axis=0)
     part = jnp.einsum("hct,cd->htd", mixed, out_weight, preferred_element_type=f32)
-    attended = tp_sum(part.astype(bf16), 3, "sum_tp_mixed")
+    attended, dd2, ga, ua = tp_sum(part.astype(bf16), 3, "sum_tp_mixed", (d2, g1, u1))
     stream = residual.astype(f32) + rounded(attended)
     normed = rms_norm(stream, norm_gain)
-    rows = comm_call(
-        tp_gather_kernel, jax.ShapeDtypeStruct((4, 2, 96, 2048), bf16), [], 13, 4, "gather_tp", (normed,)
-    ).reshape(BLOCK, 2048)
-    gate = jnp.dot(rows, gate_up[:, :width], preferred_element_type=f32)
-    upper = jnp.dot(rows, gate_up[:, width:], preferred_element_type=f32)
-    hidden = (jax.nn.silu(gate) * upper).astype(bf16)
-    down = lax.dot_general(hidden, down_all, (((1,), (1,)), ((), ())), preferred_element_type=f32)
-    summed = tp_sum(down.astype(bf16), 5, "sum_tp_down")
+    rows, gb, ub = comm_call(
+        tp_gather_kernel,
+        [
+            ((4, 2, 96, 2048), bf16, vmem()),
+            ((4, 2, *g1.shape[1:]), bf16, hbm()),
+            ((4, 3, *u1.shape[1:]), bf16, hbm()),
+        ],
+        [],
+        25,
+        4,
+        "gather_tp",
+        [(normed, vmem()), (g1, hbm()), (u1, hbm())],
+    )
+    down = feed(rows.reshape(BLOCK, 2048), g1, ga, gb, u1, ua, ub, d1, dd1, d2, dd2)
+    summed = tp_sum(down, 5, "sum_tp_down")
     return (stream + rounded(summed)).astype(bf16)
 
 

time: 254 us -> 240 us (0.945)
  Pallas kernels: 200 us -> 218 us
  matrix products: 22.9 us -> 5.86 us
  between operations: 13.6 us -> 0.17 us
    pallas_call x6 -> x7, Pallas kernels: 142 us -> 160 us  [the longest x6 145 us: comm_call(): pl.pallas_call(kernel, out_shape=[jax.ShapeDtypeStruct(shape, dtype) for...]
    dot_general x2 -> x0, matrix products: 17 us -> none  [the longest x1 11.8 us: on_device(): lax.dot_general(hidden, down_all, (((1,), (1,)), ((), ())), preferred_ele...]
  transfers between devices with their start and end apart: 2 -> 0, of which waited for: 0 -> 0; matrix products, arithmetic and copies ran while one was open for 5% -> 0% of each run, Pallas kernels for 56% -> 0%
where the time goes in v3:
time: 240 us; the launch traced here: 236 us
  Pallas kernels  218 us (91%)
  other arithmetic  6.76 us (3%)
  local copies, waits for them, and re-layouts  6.04 us (3%)
  matrix products  5.86 us (2%)
    pallas_call x6, Pallas kernels, comm_call(): pl.pallas_call(kernel, out_shape=[jax.ShapeDtypeStruct(shape, dtype) for...  145 us
    pallas_call x1, Pallas kernels, attend(): pl.pallas_call(attend_kernel, grid=(4,), in_specs=[pl.BlockSpec((4, 256,...  52.7 us
    pallas_call x1, Pallas kernels, feed(): pl.pallas_call(feed_kernel, out_shape=jax.ShapeDtypeStruct((BLOCK, 2048),...  14.2 us
    pallas_call x1, Pallas kernels, combine(): pl.pallas_call(combine_kernel, grid=(4,), in_specs=[pl.BlockSpec((4, 256,...  5.12 us

profile of v3, /device:TPU:96, one launch (start us, length us, event | category | flops | bytes accessed | tf_op | source)
XLA Modules:
  0.0 236.4 jit_solution(3976549585105874278)
XLA Ops:
  0.0 0.0 copy-start.3
  0.0 0.0 copy-start.4
  0.0 0.0 copy-start.5
  0.0 0.0 copy-start.6
  0.0 0.8 pad_maximum_fusion.2
  0.8 0.1 reshape.41
  0.9 0.7 convert_element_type.45
  1.6 0.1 copy.35
  1.7 0.1 reshape.42
  1.9 0.6 pad.4.off
  2.5 1.1 copy.30
  3.6 1.1 copy.31
  4.6 0.8 fusion.2
  5.4 0.8 fusion.4
  6.2 0.0 copy-done.3
  6.2 0.0 copy-done.4
  6.3 1.0 copy.41
  7.3 0.0 copy-start.7
  7.3 0.0 copy-done.5
  7.3 0.0 copy-done.6
  7.3 0.2 copy.40
  7.5 0.9 copy.34
  8.5 39.5 %gather_qkv.1 = (bf16[4,256,384]{2,1,0:T(8,128)(2,1)}, bf16[4,256,384]{2,1,0:T(8,128)(2,1)}, bf16[4,768,256]{2,1,0:T(8,128)(2,1)}, bf16[4,256,768]{2,1,0:T(8,128...) custom-call(bf16[256,384]{1,0:T(8,128)(2,1)} %get-tuple-element.52.q_own, ...), custom_call_target="tpu_custom_call" | custom-call | tf_op jit(solution)/shard_map/gather_qkv/pallas_call | solution.py:93
  48.0 0.0 copy-done.7
  48.0 2.2 convolution_convert_fusion.1.ext_ref
  50.2 52.7 %attend.1 = (bf16[4,256,3072]{2,1,0:T(8,128)(2,1)}, f32[16,3072]{1,0:T(8,128)}) custom-call(bf16[4,256,384]{2,1,0:T(8,128)(2,1)} %get-tuple-element.28.qa_ref, bf16[4,256,384]{2,1,0:T(8,128)(2,1)} %get-tuple-element.29.qb_ref, bf16[4,768,256]{2,1,0:T(8,128)(2,1)} %get-tuple-element.30.k_ref, bf16[4,768,128]{2,1,0:T(8,128)(2,1)} %convolution_convert_fusion.1.ext_ref, ...), custom_call_target="tpu_custom_call" | custom-call | flops 99999997952 | bytes 12000000 | tf_op jit(solution)/shard_map/attend/pallas_call | solution.py:519
  102.9 16.8 %gather_totals.1 = (f32[4,16,3072]{2,1,0:T(8,128)}, bf16[4,704,128]{2,1,0:T(8,128)(2,1)}, bf16[4,352,128]{2,1,0:T(8,128)(2,1)}) custom-call(f32[16,3072]{1,0:T(8,128)} %get-tuple-element.34.tot, bf16[704,128]{1,0:T(8,128)(2,1)} %bitcast.37, bf16[704,128]{1,0:T(8,128)(2,1)} %down.3), custom_call_target="tpu_custom_call" | custom-call | tf_op jit(solution)/shard_map/gather_totals/pallas_call | solution.py:93
  119.7 5.1 %combine.1 = (bf16[4,256,384]{2,1,0:T(8,128)(2,1)}, bf16[4,256,384]{2,1,0:T(8,128)(2,1)}) custom-call(bf16[4,256,3072]{2,1,0:T(8,128)(2,1)} %get-tuple-element.33.oa_ref.ob_ref, bf16[4,256,3072]{2,1,0:T(8,128)(2,1)} %get-tuple-element.33.oa_ref.ob_ref, f32[4,16,3072]{2,1,0:T(8,128)} %get-tuple-element.35.ta_ref.tb_ref, ...), custom_call_target="tpu_custom_call" | custom-call | flops 6291456 | bytes 9000000 | tf_op jit(solution)/shard_map/combine/pallas_call | solution.py:576
  124.9 0.0 copy-start.1
  124.9 0.0 copy-start.2
  124.9 19.6 %sum_x.1 = (bf16[2,256,384]{2,1,0:T(8,128)(2,1)}, bf16[4,4,352,128]{3,2,1,0:T(8,128)(2,1)}) custom-call(bf16[4,256,384]{2,1,0:T(8,128)(2,1)} %get-tuple-element.36.parts_a, bf16[4,256,384]{2,1,0:T(8,128)(2,1)} %get-tuple-element.37.parts_b, bf16[4,352,128]{2,1,0:T(8,128)(2,1)} %get-tuple-element.38.d1), custom_call_target="tpu_custom_call" | custom-call | tf_op jit(solution)/shard_map/sum_x/pallas_call | solution.py:93
  144.5 0.0 copy-done.1
  144.5 0.0 copy-done.2
  144.5 3.6 %convolution_convert_fusion = bf16[2,384,2048]{2,1,0:T(8,128)(2,1)} fusion(bf16[2,256,384]{2,1,0:T(8,128)(2,1)} %get-tuple-element.39, bf16[128,2048]{1,0:T(8,128)(2,1)S(1)} %copy-done.1, bf16[128,2048]{1,0:T(8,128)(2,1)S(1)} %copy-done.2), kind=kOutput, calls=%fused_computation | convolution fusion | flops 808976384 | bytes 4587520 | tf_op jit(solution)/shard_map/hct,cd->htd/dot_general | solution.py:793
  148.2 0.0 copy-start
  148.2 23.5 %sum_tp_mixed.1 = (f32[96,2048]{1,0:T(8,128)}, bf16[4,4,352,128]{3,2,1,0:T(8,128)(2,1)}, bf16[4,2,704,128]{3,2,1,0:T(8,128)(2,1)}, bf16[4,1,704,128]{3,2,1,0:T(8,128)(2,1)}) custom-call(bf16[4,2,96,2048]{3,2,1,0:T(8,128)(2,1)} %bitcast.28, bf16[4,352,128]{2,1,0:T(8,128)(2,1)} %get-tuple-element.40.refs_1_.d2, ...), custom_call_target="tpu_custom_call" | custom-call | tf_op jit(solution)/shard_map/sum_tp_mixed/pallas_call | solution.py:93
  171.7 1.2 convert_element_type.43
  172.8 0.0 copy-done
  172.9 0.2 multiply_reduce_fusion
  173.1 0.9 multiply_convert_fusion.own
  174.0 25.3 %gather_tp.1 = (bf16[4,2,96,2048]{3,2,1,0:T(8,128)(2,1)}, bf16[4,2,704,128]{3,2,1,0:T(8,128)(2,1)}, bf16[4,3,704,128]{3,2,1,0:T(8,128)(2,1)}) custom-call(bf16[96,2048]{1,0:T(8,128)(2,1)} %multiply_convert_fusion.own, bf16[4,704,128]{2,1,0:T(8,128)(2,1)} %get-tuple-element.41.refs_2_.g1, bf16[4,704,128]{2,1,0:T(8,128)(2,1)} %get-tuple-element.42.refs_3_.u1), custom_call_target="tpu_custom_call" | custom-call | tf_op jit(solution)/shard_map/gather_tp/pallas_call | solution.py:93
  199.4 14.2 %feed.1 = bf16[768,2048]{1,0:T(8,128)(2,1)} custom-call(bf16[768,2048]{1,0:T(8,128)(2,1)} %bitcast.38, bf16[4,704,128]{2,1,0:T(8,128)(2,1)} %get-tuple-element.41.refs_2_.g1, bf16[4,2,704,128]{3,2,1,0:T(8,128)(2,1)} %get-tuple-element.45.ga, bf16[4,2,704,128]{3,2,1,0:T(8,128)(2,1)} %get-tuple-element.46.gb, ...), custom_call_target="tpu_custom_call" | custom-call | flops 6643777536 | bytes 15000000 | tf_op jit(solution)/shard_map/feed/pallas_call | solution.py:689
  213.6 20.7 %sum_tp_down.1 = f32[96,2048]{1,0:T(8,128)} custom-call(bf16[4,2,96,2048]{3,2,1,0:T(8,128)(2,1)} %bitcast.29), custom_call_target="tpu_custom_call" | custom-call | tf_op jit(solution)/shard_map/sum_tp_down/pallas_call | solution.py:93
  234.3 1.2 convert_element_type.47
  235.5 0.9 add_convert_fusion
  (3 shorter events, 0.1 us)
Async XLA Ops:
  0.0 6.2 %copy-start.3 = (bf16[768,128]{1,0:T(8,128)(2,1)S(1)}, bf16[768,128]{1,0:T(8,128)(2,1)}, u32[]{:S(2)}) copy-start(bf16[768,128]{1,0:T(8,128)(2,1)} %param.22) | copy-start | bytes 589828
  0.0 6.2 %copy-start.4 = (bf16[768,128]{1,0:T(8,128)(2,1)S(1)}, bf16[768,128]{1,0:T(8,128)(2,1)}, u32[]{:S(2)}) copy-start(bf16[768,128]{1,0:T(8,128)(2,1)} %param.18) | copy-start | bytes 589828
  0.0 7.3 %copy-start.5 = (bf16[768,128]{1,0:T(8,128)(2,1)S(1)}, bf16[768,128]{1,0:T(8,128)(2,1)}, u32[]{:S(2)}) copy-start(bf16[768,128]{1,0:T(8,128)(2,1)} %param.23) | copy-start | bytes 589828
  0.0 7.3 %copy-start.6 = (bf16[768,128]{1,0:T(8,128)(2,1)S(1)}, bf16[768,128]{1,0:T(8,128)(2,1)}, u32[]{:S(2)}) copy-start(bf16[768,128]{1,0:T(8,128)(2,1)} %param.19) | copy-start | bytes 589828
  7.3 40.7 %copy-start.7 = (bf16[32,128,1]{1,0,2:T(8,128)(2,1)S(1)}, bf16[32,128,1]{1,0,2:T(8,128)(2,1)}, u32[]{:S(2)}) copy-start(bf16[32,128,1]{1,0,2:T(8,128)(2,1)} %constant.21) | copy-start | bytes 24580
  124.9 19.6 %copy-start.1 = (bf16[128,2048]{1,0:T(8,128)(2,1)S(1)}, bf16[128,2048]{1,0:T(8,128)(2,1)}, u32[]{:S(2)}) copy-start(bf16[128,2048]{1,0:T(8,128)(2,1)} %param.26) | copy-start | bytes 1572868
  124.9 19.6 %copy-start.2 = (bf16[128,2048]{1,0:T(8,128)(2,1)S(1)}, bf16[128,2048]{1,0:T(8,128)(2,1)}, u32[]{:S(2)}) copy-start(bf16[128,2048]{1,0:T(8,128)(2,1)} %param.25) | copy-start | bytes 1572868
  148.2 24.7 %copy-start = (bf16[96,2048]{1,0:T(8,128)(2,1)S(1)}, bf16[96,2048]{1,0:T(8,128)(2,1)}, u32[]{:S(2)}) copy-start(bf16[96,2048]{1,0:T(8,128)(2,1)} %param.27) | copy-start | bytes 1179652

commit v4 on v3

--- a/solution.py
+++ b/solution.py
@@ -196,30 +196,6 @@
     copies.drain_sends()
 
 
-def totals_kernel(tot, up, down, tot_all, u1, d2, keep_sems, send_sems, recv_sems):
-    z, x = sp_coords()
-    zs, xs = z_neighbours(), x_neighbours()
-    greet((*zs, *xs))
-    copies, keep = Copies(send_sems, recv_sems), Keep(keep_sems)
-    second = down.at[pl.ds(down.shape[0] // 2, down.shape[0] // 2)]
-    jobs = [
-        RingGather(copies, tot, tot_all, x, xs),
-        RingGather(copies, up, u1, z, zs),
-        RingGather(copies, second, d2, z, zs),
-    ]
-    for job in jobs:
-        job.start()
-    keep.start(up, u1.at[z])
-    keep.start(second, d2.at[z])
-    tot_all[x] = tot[...]
-    for job in jobs:
-        job.pass_on()
-    for job in jobs:
-        job.finish()
-    keep.finish()
-    copies.drain_sends()
-
-
 def plus(a, b):
     return (a.astype(jnp.float32) + b.astype(jnp.float32)).astype(jnp.bfloat16)
 
@@ -270,143 +246,192 @@
         return own + self.arrived[0].astype(jnp.float32) + self.arrived[1].astype(jnp.float32)
 
 
-def x_sum_kernel(
-    parts_a, parts_b, d1, out, dd1, pa, pb, relay_a, relay_b, arrived_a, arrived_b, give, got, send_sems, recv_sems
+def scaled(o_ref, tot_ref, x, columns):
+    nearer = jnp.zeros((4, HALF), jnp.float32)
+    factors = [None] * 4
+    for kb in reversed(range(4)):
+        here = jnp.zeros((4, HALF), jnp.float32)
+        block = jnp.zeros((4, HALF), jnp.float32)
+        for other in range(4):
+            term = tot_ref[other, kb * 4 : kb * 4 + 4, columns]
+            block = block + term
+            here = here + jnp.where(other > x, term, 0.0)
+        factors[kb] = jnp.exp2(-(nearer + here))
+        nearer = nearer + block
+    pieces = []
+    for head, _, row, size in HEADS:
+        total = jnp.zeros((size, HALF), jnp.float32)
+        for kb in range(4):
+            term = o_ref[kb, row : row + size, columns].astype(jnp.float32)
+            total = total + term * factors[kb][head : head + 1]
+        pieces.append(total)
+    return jnp.concatenate(pieces, axis=0)
+
+
+def mix_kernel(
+    tot, up, down, o_hbm, out, u1, d2, tot_all, o_ref, pa, pb, relay_a, relay_b, arrived_a, arrived_b, give, got,
+    keep_sems, load_sems, send_sems, recv_sems,
 ):
     z, x = sp_coords()
-    right, left = x_neighbours()
-    zs = z_neighbours()
-    greet((right, left, *zs))
-    copies = Copies(send_sems, recv_sems)
-    weights = RingGather(copies, d1, dd1, z, zs, by_units)
-    weights.start()
-    rings = []
-    for source, parts, relay, arrived in (
-        (parts_b, pb, relay_b, arrived_b), (parts_a, pa, relay_a, arrived_a)
-    ):
-        ring = RingSum(copies, parts, relay, arrived, x, right, left, 256)
-        parts[...] = source[...]
-        ring.send_far()
-        ring.send_after()
-        ring.send_before()
-        rings.append(ring)
+    zs, xs = z_neighbours(), x_neighbours()
+    greet((*zs, *xs))
+    copies, keep = Copies(send_sems, recv_sems), Keep(keep_sems)
+    second = down.at[pl.ds(down.shape[0] // 2, down.shape[0] // 2)]
+    totals = RingGather(copies, tot, tot_all, x, xs)
+    weights = [RingGather(copies, up, u1, z, zs), RingGather(copies, second, d2, z, zs)]
+    totals.start()
+    for job in weights:
+        job.start()
+    keep.start(up, u1.at[z])
+    keep.start(second, d2.at[z])
+    rings = [
+        RingSum(copies, parts, relay, arrived, x, *xs, 256)
+        for parts, relay, arrived in ((pb, relay_b, arrived_b), (pa, relay_a, arrived_a))
+    ]
+
+    def columns(group, place):
+        return pl.ds(pl.multiple_of((group * 4 + place) * HALF, 128), HALF)
+
+    loads = {}
+    for n, (ring, group) in enumerate(zip(rings, (1, 0))):
+        for m, place in enumerate((ring.far, ring.after, ring.before, x)):
+            span = columns(group, place)
+            loads[n, m] = pltpu.make_async_copy(
+                o_hbm.at[:, :, span], o_ref.at[:, :, span], load_sems.at[n * 4 + m]
+            )
+            loads[n, m].start()
+    tot_all[x] = tot[...]
+    totals.pass_on()
+    totals.finish()
+    for n, (ring, group) in enumerate(zip(rings, (1, 0))):
+        sends = (ring.send_far, ring.send_after, ring.send_before)
+        for m, (place, send) in enumerate(zip((ring.far, ring.after, ring.before), sends)):
+            loads[n, m].wait()
+            ring.parts[place] = scaled(o_ref, tot_all, x, columns(group, place)).astype(jnp.bfloat16)
+            send()
+    for job in weights:
+        job.pass_on()
     for ring in rings:
         ring.pass_on()
-    weights.pass_on()
-    give[...] = rings[0].finish(pb[x].astype(jnp.float32)).astype(jnp.bfloat16)
+    loads[0, 3].wait()
+    give[...] = rings[0].finish(scaled(o_ref, tot_all, x, columns(1, x))).astype(jnp.bfloat16)
     swap = copies.make(give, got, mirror())
     swap.start()
-    out[0] = rings[1].finish(pa[x].astype(jnp.float32)).astype(jnp.bfloat16)
+    loads[1, 3].wait()
+    out[0] = rings[1].finish(scaled(o_ref, tot_all, x, columns(0, x))).astype(jnp.bfloat16)
+    for job in weights:
+        job.finish()
+    keep.finish()
     swap.wait_recv()
     out[1] = got[...]
-    weights.finish()
     copies.drain_sends()
 
 
-def tp_sum_kernel(with_weights, *refs):
-    if with_weights:
-        terms, d2, g1, u1, out, dd2, ga, ua, other, parts, relay, arrived, send_sems, recv_sems = refs
-    else:
-        terms, out, other, parts, relay, arrived, send_sems, recv_sems = refs
-    t = lax.axis_index("tp")
-    y, core = t // 2, t % 2
-    right, left = y_neighbours()
-    mate = sibling()
-    z, x = sp_coords()
-    zs, xs = z_neighbours(), x_neighbours()
-    greet((right, left, mate, *zs, *xs) if with_weights else (right, left, mate))
-    copies = Copies(send_sems, recv_sems)
-    weights = []
-    if with_weights:
-        weights = [
-            RingGather(copies, d2, dd2, x, xs, by_units),
-            RingGather(copies, g1.at[pl.ds(0, 2)], ga, z, zs, by_units),
-            RingGather(copies, u1.at[pl.ds(0, 1)], ua, x, xs),
-        ]
-    ring = RingSum(copies, parts, relay, arrived, y, right, left, 96)
+def pair_sum(copies, terms, other, ring, y, core, mate):
     order = (ring.far, ring.after, ring.before, y)
     given = []
     for place in order:
         copy = copies.make(terms.at[place, 1 - core], other.at[place], mate)
         copy.start()
         given.append(copy)
-    for job in weights:
-        job.start()
     for place, copy, then in zip(order, given, (ring.send_far, ring.send_after, ring.send_before)):
         copy.wait_recv()
-        parts[place] = plus(terms[place, core], other[place])
+        ring.parts[place] = plus(terms[place, core], other[place])
         then()
     ring.pass_on()
-    for job in weights:
+    given[3].wait_recv()
+    return terms[y, core].astype(jnp.float32) + other[y].astype(jnp.float32)
+
+
+def tp_place():
+    t = lax.axis_index("tp")
+    return t // 2, t % 2
+
+
+def tp_sum_kernel(terms, out, other, parts, relay, arrived, send_sems, recv_sems):
+    y, core = tp_place()
+    ys, mate = y_neighbours(), sibling()
+    greet((*ys, mate))
+    copies = Copies(send_sems, recv_sems)
+    ring = RingSum(copies, parts, relay, arrived, y, *ys, 96)
+    own = pair_sum(copies, terms, other, ring, y, core, mate)
+    out[...] = ring.finish(own)
+    copies.drain_sends()
+
+
+def middle_kernel(
+    terms, residual, gain, d1, d2, g1, u1, stream, whole, dd1, dd2, gg, uu, other, parts, relay, arrived, own,
+    send_sems, recv_sems,
+):
+    z, x = sp_coords()
+    y, core = tp_place()
+    zs, xs, ys, mate = z_neighbours(), x_neighbours(), y_neighbours(), sibling()
+    greet((*ys, mate, *zs, *xs))
+    copies = Copies(send_sems, recv_sems)
+    early = [
+        RingGather(copies, d2, dd2, x, xs, by_units),
+        RingGather(copies, d1, dd1, z, zs, by_units),
+    ]
+    late = [
+        RingGather(copies, u1, uu, x, xs, by_units),
+        RingGather(copies, g1, gg, z, zs, by_units),
+    ]
+    ring = RingSum(copies, parts, relay, arrived, y, *ys, 96)
+    for job in early + late:
+        job.start()
+    total = pair_sum(copies, terms, other, ring, y, core, mate)
+    for job in early:
         job.pass_on()
-    given[3].wait_recv()
-    own = terms[y, core].astype(jnp.float32) + other[y].astype(jnp.float32)
-    out[...] = ring.finish(own)
-    for job in weights:
-        job.finish()
-    copies.drain_sends()
-
-
-def tp_gather_kernel(own, g1, u1, whole, gb, ub, send_sems, recv_sems):
-    t = lax.axis_index("tp")
-    y, core = t // 2, t % 2
-    right, left = y_neighbours()
-    mate = sibling()
-    z, x = sp_coords()
-    zs, xs = z_neighbours(), x_neighbours()
-    greet((right, left, mate, *zs, *xs))
-    copies = Copies(send_sems, recv_sems)
-    weights = [
-        RingGather(copies, g1.at[pl.ds(2, 2)], gb, z, zs, by_units),
-        RingGather(copies, u1.at[pl.ds(1, 3)], ub, x, xs),
-    ]
+    attended = ring.finish(total).astype(jnp.bfloat16).astype(jnp.float32)
+    value = residual[...].astype(jnp.float32) + attended
+    stream[...] = value
+    scale = lax.rsqrt(jnp.mean(value * value, axis=-1, keepdims=True) + 1e-06)
+    own[...] = (value * scale * gain[...].astype(jnp.float32)).astype(jnp.bfloat16)
+
+    right, left = ys
     before, after, far = (y + 3) % 4, (y + 1) % 4, (y + 2) % 4
     top, low = pl.ds(0, 48), pl.ds(48, 48)
-    mine = whole.at[y, core]
     sent = (
         copies.make(own.at[top], whole.at[y, core, top], right),
         copies.make(own.at[low], whole.at[y, core, low], left),
         copies.make(own.at[low], whole.at[y, core, low], right),
         copies.make(own.at[top], whole.at[y, core, top], left),
-        copies.make(own, mine, mate),
+        copies.make(own, whole.at[y, core], mate),
     )
     for copy in sent:
         copy.start()
-    for job in weights:
-        job.start()
     whole[y, core] = own[...]
     over = [sent[4]]
 
-    def across(block):
-        copy = copies.make(block, block, mate)
+    def send(block, device):
+        copy = copies.make(block, block, device)
         copy.start()
-        over.append(copy)
+        return copy
 
     sent[0].wait_recv()
-    first = whole.at[before, core, top]
-    on_right = copies.make(first, first, right)
-    on_right.start()
-    across(first)
+    on_right = send(whole.at[before, core, top], right)
+    over.append(send(whole.at[before, core, top], mate))
     sent[1].wait_recv()
-    second = whole.at[after, core, low]
-    on_left = copies.make(second, second, left)
-    on_left.start()
-    across(second)
+    on_left = send(whole.at[after, core, low], left)
+    over.append(send(whole.at[after, core, low], mate))
+    for job in late:
+        job.pass_on()
     sent[2].wait_recv()
-    across(whole.at[before, core, low])
+    over.append(send(whole.at[before, core, low], mate))
     sent[3].wait_recv()
-    across(whole.at[after, core, top])
-    for job in weights:
-        job.pass_on()
+    over.append(send(whole.at[after, core, top], mate))
     on_right.wait_recv()
-    across(whole.at[far, core, top])
+    over.append(send(whole.at[far, core, top], mate))
     on_left.wait_recv()
-    across(whole.at[far, core, low])
+    over.append(send(whole.at[far, core, low], mate))
     for copy in over:
         copy.wait_recv()
-    for job in weights:
+    for job in early + late:
         job.finish()
     copies.drain_sends()
+
+
+HEADS = ((0, 0, 0, 64), (1, 0, 64, 64), (2, 128, 128, 128))
 
 
 def selector(head):
@@ -420,9 +445,6 @@
     for n, piece in enumerate(pieces):
         value = jnp.where(rows == 3 * head + n, piece, value)
     return value.astype(jnp.bfloat16)
-
-
-HEADS = ((0, 0, 0, 64), (1, 0, 64, 64), (2, 128, 128, 128))
 
 
 def attend_kernel(qa_ref, qb_ref, k_ref, ext_ref, v_ref, o_ref, tot_ref, work_ref, rhs_ref):
@@ -548,81 +570,31 @@
     )(qa, qb, k_all, ext, v_all)
 
 
-def combine_kernel(oa_ref, ob_ref, ta_ref, tb_ref, outa_ref, outb_ref):
-    _, x = sp_coords()
-    for o_ref, tot_ref, out_ref in ((oa_ref, ta_ref, outa_ref), (ob_ref, tb_ref, outb_ref)):
-        nearer = jnp.zeros((4, HALF), jnp.float32)
-        factors = [None] * 4
-        for kb in reversed(range(4)):
-            rows = slice(kb * 4, kb * 4 + 4)
-            here = jnp.zeros((4, HALF), jnp.float32)
-            block = jnp.zeros((4, HALF), jnp.float32)
-            for other in range(4):
-                term = tot_ref[other, rows, :]
-                block = block + term
-                here = here + jnp.where(other > x, term, 0.0)
-            factors[kb] = jnp.exp2(-(nearer + here))
-            nearer = nearer + block
-        for head, _, row, size in HEADS:
-            total = jnp.zeros((size, HALF), jnp.float32)
-            for kb in range(4):
-                term = o_ref[kb, row : row + size, :].astype(jnp.float32)
-                total = total + term * factors[kb][head : head + 1]
-            out_ref[0, row : row + size, :] = total.astype(jnp.bfloat16)
-
-
-def combine(outs, totals):
-    half = jax.ShapeDtypeStruct((4, 256, HALF), jnp.bfloat16)
-    return pl.pallas_call(
-        combine_kernel,
-        grid=(4,),
-        in_specs=[
-            pl.BlockSpec((4, 256, HALF), lambda i: (0, 0, i)),
-            pl.BlockSpec((4, 256, HALF), lambda i: (0, 0, i + 4)),
-            pl.BlockSpec((4, 16, HALF), lambda i: (0, 0, i)),
-            pl.BlockSpec((4, 16, HALF), lambda i: (0, 0, i + 4)),
-        ],
-        out_specs=[pl.BlockSpec((1, 256, HALF), lambda i: (i, 0, 0))] * 2,
-        out_shape=[half, half],
-        compiler_params=pltpu.CompilerParams(dimension_semantics=("arbitrary",)),
-        cost_estimate=pl.CostEstimate(
-            flops=4 * 256 * 3072 * 2, bytes_accessed=9_000_000, transcendentals=50_000
-        ),
-        name="combine",
-    )(outs, outs, totals, totals)
-
-
-def tp_sum(terms, collective_id, name, weights=()):
+def sum_scratch(shape):
+    bf16 = jnp.bfloat16
+    return [
+        pltpu.VMEM((4, *shape), bf16),
+        pltpu.VMEM((4, *shape), bf16),
+        pltpu.VMEM((2, shape[0] // 2, shape[1]), bf16),
+        pltpu.VMEM((2, *shape), bf16),
+    ]
+
+
+def tp_sum(terms, collective_id, name):
     shape = (96, terms.shape[-1])
-    bf16 = jnp.bfloat16
-    outs, args = [(shape, jnp.float32, vmem())], [(terms.reshape(4, 2, *shape), vmem())]
-    if weights:
-        d2, g1, u1 = weights
-        args += [(array, hbm()) for array in weights]
-        outs += [
-            ((4, *d2.shape), bf16, hbm()),
-            ((4, 2, *g1.shape[1:]), bf16, hbm()),
-            ((4, 1, *u1.shape[1:]), bf16, hbm()),
-        ]
-    out = comm_call(
-        functools.partial(tp_sum_kernel, bool(weights)),
-        outs,
-        [
-            pltpu.VMEM((4, *shape), bf16),
-            pltpu.VMEM((4, *shape), bf16),
-            pltpu.VMEM((2, 48, shape[1]), bf16),
-            pltpu.VMEM((2, *shape), bf16),
-        ],
-        28 if weights else 10,
+    return comm_call(
+        tp_sum_kernel,
+        [(shape, jnp.float32, vmem())],
+        sum_scratch(shape),
+        10,
         collective_id,
         name,
-        args,
-    )
-    return out if weights else out[0]
+        [(terms.reshape(4, 2, *shape), vmem())],
+    )[0]
 
 
 def feed_kernel(
-    rows, g1, ga, gb, u1, ua, ub, d1, dd1, d2, dd2, out, r_vmem, gate_w, up_w, down_w, gate, hidden, sems
+    rows, g1, gg, u1, uu, d1, dd1, d2, dd2, out, r_vmem, gate_w, up_w, down_w, gate, hidden, sems
 ):
     z, x = sp_coords()
     half = d1.shape[1]
@@ -639,10 +611,9 @@
 
     spots = [(zp, xp, pl.ds((zp * 4 + xp) * 128, 128)) for zp in range(4) for xp in range(4)]
     for n, (zp, xp, lanes) in enumerate(spots):
-        fetch(0, z == zp, g1.at[xp], (ga, gb)[xp // 2].at[zp, xp % 2], gate_w.at[:, lanes], n)
+        fetch(0, z == zp, g1.at[xp], gg.at[zp, xp], gate_w.at[:, lanes], n)
     for n, (zp, xp, lanes) in enumerate(spots):
-        other = ua.at[xp, 0] if zp == 0 else ub.at[xp, zp - 1]
-        fetch(1, x == xp, u1.at[zp], other, up_w.at[:, lanes], 16 + n)
+        fetch(1, x == xp, u1.at[zp], uu.at[xp, zp], up_w.at[:, lanes], 16 + n)
     for n, (zp, xp, lanes) in enumerate(spots):
         fetch(2, z == zp, d1.at[xp], dd1.at[zp, xp], down_w.at[pl.ds(0, half), lanes], 32 + n)
         fetch(2, x == xp, d2.at[zp], dd2.at[xp, zp], down_w.at[pl.ds(half, half), lanes], 48 + n)
@@ -710,11 +681,6 @@
 
 def rounded(value):
     return lax.optimization_barrier(value.astype(jnp.bfloat16)).astype(jnp.float32)
-
-
-def rms_norm(stream, gain):
-    scale = lax.rsqrt(jnp.mean(stream * stream, axis=-1, keepdims=True) + 1e-06)
-    return (stream * scale * gain.astype(jnp.float32)).astype(jnp.bfloat16)
 
 
 def striped(value):
@@ -762,53 +728,46 @@
         "bhs,hc->bsc", off_all, jnp.asarray(spread, bf16), preferred_element_type=f32
     ).astype(bf16)
     outs, totals = attend(qa_all, qb_all, k_all, ext, v_all)
-    totals, u1, d2 = comm_call(
-        totals_kernel,
+    half = (256, HALF)
+    buffers = [pltpu.VMEM((4, 16, 4 * BLOCK), f32), pltpu.VMEM((4, 256, 4 * BLOCK), bf16)]
+    for shape in ((4, *half), (2, 128, HALF), (2, *half), half):
+        buffers += [pltpu.VMEM(shape, bf16)] * 2
+    mixed, u1, d2 = comm_call(
+        mix_kernel,
         [
-            ((4, 16, 4 * BLOCK), f32, vmem()),
+            ((2, *half), bf16, vmem()),
             ((4, units, 128), bf16, hbm()),
             ((4, units // 2, 128), bf16, hbm()),
         ],
-        [pltpu.SemaphoreType.DMA((2,))],
-        18,
+        [*buffers, pltpu.SemaphoreType.DMA((2,)), pltpu.SemaphoreType.DMA((8,))],
+        31,
         1,
-        "gather_totals",
-        [(array, vmem()) for array in (totals, up, down)],
-    )
-    parts_a, parts_b = combine(outs, totals)
-    buffers = [pltpu.VMEM((256, HALF), bf16)] * 2
-    for shape in ((4, 256, HALF), (2, 128, HALF), (2, 256, HALF)):
-        buffers = [pltpu.VMEM(shape, bf16)] * 2 + buffers
-    buffers = buffers[4:6] + buffers[2:4] + buffers[0:2] + buffers[6:]
-    mixed, dd1 = comm_call(
-        x_sum_kernel,
-        [((2, 256, HALF), bf16, vmem()), ((4, *d1.shape), bf16, hbm())],
-        buffers,
-        19,
-        2,
-        "sum_x",
-        [(parts_a, vmem()), (parts_b, vmem()), (d1, hbm())],
+        "mix",
+        [(totals, vmem()), (up, vmem()), (down, vmem()), (outs, hbm())],
     )
     out_weight = jnp.concatenate([out_small, out_large], axis=0)
     part = jnp.einsum("hct,cd->htd", mixed, out_weight, preferred_element_type=f32)
-    attended, dd2, ga, ua = tp_sum(part.astype(bf16), 3, "sum_tp_mixed", (d2, g1, u1))
-    stream = residual.astype(f32) + rounded(attended)
-    normed = rms_norm(stream, norm_gain)
-    rows, gb, ub = comm_call(
-        tp_gather_kernel,
+    shape = (96, part.shape[-1])
+    terms = part.astype(bf16).reshape(4, 2, *shape)
+    stream, rows, dd1, dd2, gg, uu = comm_call(
+        middle_kernel,
         [
-            ((4, 2, 96, 2048), bf16, vmem()),
-            ((4, 2, *g1.shape[1:]), bf16, hbm()),
-            ((4, 3, *u1.shape[1:]), bf16, hbm()),
-        ],
-        [],
-        25,
-        4,
-        "gather_tp",
-        [(normed, vmem()), (g1, hbm()), (u1, hbm())],
+            (shape, f32, vmem()),
+            ((4, 2, *shape), bf16, vmem()),
+            ((4, *d1.shape), bf16, hbm()),
+            ((4, *d2.shape), bf16, hbm()),
+            ((4, *g1.shape), bf16, hbm()),
+            ((4, *u1.shape), bf16, hbm()),
+        ],
+        [*sum_scratch(shape), pltpu.VMEM(shape, bf16)],
+        47,
+        3,
+        "middle",
+        [(terms, vmem()), (residual, vmem()), (norm_gain.reshape(1, -1), vmem())]
+        + [(array, hbm()) for array in (d1, d2, g1, u1)],
     )
-    down = feed(rows.reshape(BLOCK, 2048), g1, ga, gb, u1, ua, ub, d1, dd1, d2, dd2)
-    summed = tp_sum(down, 5, "sum_tp_down")
+    down_terms = feed(rows.reshape(BLOCK, 2048), g1, gg, u1, uu, d1, dd1, d2, dd2)
+    summed = tp_sum(down_terms, 5, "sum_tp_down")
     return (stream + rounded(summed)).astype(bf16)
 
 

time: 240 us -> 224 us (0.933)
  Pallas kernels: 218 us -> 203 us
    pallas_call x6 -> x4, Pallas kernels: 145 us -> 136 us  [comm_call(): pl.pallas_call(kernel, out_shape=[jax.ShapeDtypeStruct(shape, dtype) for...]
    pallas_call x1 -> x0, Pallas kernels: 5.12 us -> none  [combine(): pl.pallas_call(combine_kernel, grid=(4,), in_specs=[pl.BlockSpec((4, 256,...]
where the time goes in v4:
time: 224 us; the launch traced here: 221 us
  Pallas kernels  203 us (91%)
  local copies, waits for them, and re-layouts  7.34 us (3%)
  matrix products  5.93 us (3%)
  other arithmetic  4.7 us (2%)
    pallas_call x4, Pallas kernels, comm_call(): pl.pallas_call(kernel, out_shape=[jax.ShapeDtypeStruct(shape, dtype) for...  136 us
    pallas_call x1, Pallas kernels, attend(): pl.pallas_call(attend_kernel, grid=(4,), in_specs=[pl.BlockSpec((4, 256,...  52.7 us
    pallas_call x1, Pallas kernels, feed(): pl.pallas_call(feed_kernel, out_shape=jax.ShapeDtypeStruct((BLOCK, 2048),...  14.1 us

profile of v4, /device:TPU:96, one launch (start us, length us, event | category | flops | bytes accessed | tf_op | source)
XLA Modules:
  0.0 221.0 jit_solution(15629614594333779019)
XLA Ops:
  0.0 0.0 copy-start.3
  0.0 0.0 copy-start.4
  0.0 0.8 pad_maximum_fusion.2
  0.8 0.1 reshape.35
  0.9 1.3 reshape.38.gain
  2.1 0.1 copy.35
  2.3 0.1 reshape.36
  2.4 0.6 pad.4.off
  3.0 1.1 copy.30
  4.1 1.1 copy.31
  5.2 0.8 fusion.2
  6.0 0.8 fusion.4
  6.8 0.0 copy-start.5
  6.8 1.1 pad_maximum_fusion
  7.9 1.0 copy.41
  8.8 0.0 copy-done.3
  8.9 0.0 copy-done.4
  8.9 0.2 copy.40
  9.1 0.9 copy.34
  10.1 39.5 %gather_qkv.1 = (bf16[4,256,384]{2,1,0:T(8,128)(2,1)}, bf16[4,256,384]{2,1,0:T(8,128)(2,1)}, bf16[4,768,256]{2,1,0:T(8,128)(2,1)}, bf16[4,256,768]{2,1,0:T(8,128...) custom-call(bf16[256,384]{1,0:T(8,128)(2,1)} %get-tuple-element.42.q_own, ...), custom_call_target="tpu_custom_call" | custom-call | tf_op jit(solution)/shard_map/gather_qkv/pallas_call | solution.py:93
  49.6 0.0 copy-done.5
  49.6 2.2 %convolution_convert_fusion.1.ext_ref = bf16[4,768,128]{2,1,0:T(8,128)(2,1)} fusion(bf16[4,32,768]{2,1,0:T(8,128)(2,1)} %get-tuple-element.26, bf16[32,128,1]{1,0,2:T(8,128)(2,1)S(1)} %copy-done.5), kind=kOutput, calls=%fused_computation.1 | convolution fusion | flops 25559040 | bytes 991232 | tf_op jit(solution)/shard_map/bhs,hc->bsc/dot_general | solution.py:727
  51.9 52.7 %attend.1 = (bf16[4,256,3072]{2,1,0:T(8,128)(2,1)}, f32[16,3072]{1,0:T(8,128)}) custom-call(bf16[4,256,384]{2,1,0:T(8,128)(2,1)} %get-tuple-element.23.qa_ref, bf16[4,256,384]{2,1,0:T(8,128)(2,1)} %get-tuple-element.24.qb_ref, bf16[4,768,256]{2,1,0:T(8,128)(2,1)} %get-tuple-element.25.k_ref, bf16[4,768,128]{2,1,0:T(8,128)(2,1)} %convolution_convert_fusion.1.ext_ref, ...), custom_call_target="tpu_custom_call" | custom-call | flops 99999997952 | bytes 12000000 | tf_op jit(solution)/shard_map/attend/pallas_call | solution.py:541
  104.6 0.0 copy-start.1
  104.6 0.0 copy-start.2
  104.6 30.7 %mix.1 = (bf16[2,256,384]{2,1,0:T(8,128)(2,1)}, bf16[4,704,128]{2,1,0:T(8,128)(2,1)}, bf16[4,352,128]{2,1,0:T(8,128)(2,1)}) custom-call(f32[16,3072]{1,0:T(8,128)} %get-tuple-element.28.tot, bf16[704,128]{1,0:T(8,128)(2,1)} %bitcast.37, bf16[704,128]{1,0:T(8,128)(2,1)} %down.3, bf16[4,256,3072]{2,1,0:T(8,128)(2,1)} %get-tuple-element.29.o_hbm), custom_call_target="tpu_custom_call" | custom-call | tf_op jit(solution)/shard_map/mix/pallas_call | solution.py:93
  135.3 0.0 copy-done.1
  135.3 0.0 copy-done.2
  135.3 3.7 %convolution_convert_fusion = bf16[2,384,2048]{2,1,0:T(8,128)(2,1)} fusion(bf16[2,256,384]{2,1,0:T(8,128)(2,1)} %get-tuple-element.30, bf16[128,2048]{1,0:T(8,128)(2,1)S(1)} %copy-done.1, bf16[128,2048]{1,0:T(8,128)(2,1)S(1)} %copy-done.2), kind=kOutput, calls=%fused_computation | convolution fusion | flops 808976384 | bytes 4587520 | tf_op jit(solution)/shard_map/hct,cd->htd/dot_general | solution.py:749
  139.0 43.7 %middle.1 = (f32[96,2048]{1,0:T(8,128)}, bf16[4,2,96,2048]{3,2,1,0:T(8,128)(2,1)}, bf16[4,4,352,128]{3,2,1,0:T(8,128)(2,1)}, bf16[4,4,352,128]{3,2,1,0:T(8,128)(...) custom-call(bf16[4,2,96,2048]{3,2,1,0:T(8,128)(2,1)} %bitcast.28, bf16[96,2048]{1,0:T(8,128)(2,1)} %residual.1, ...), custom_call_target="tpu_custom_call" | custom-call | tf_op jit(solution)/shard_map/middle/pallas_call | solution.py:93
  182.8 14.1 %feed.1 = bf16[768,2048]{1,0:T(8,128)(2,1)} custom-call(bf16[768,2048]{1,0:T(8,128)(2,1)} %bitcast.38, bf16[4,704,128]{2,1,0:T(8,128)(2,1)} %get-tuple-element.33.g1, bf16[4,4,704,128]{3,2,1,0:T(8,128)(2,1)} %get-tuple-element.37.gg, bf16[4,704,128]{2,1,0:T(8,128)(2,1)} %get-tuple-element.34.u1, bf16[4,4,704,128]{3,2,1,0:T(8,128)(2,1)} %get-tuple-element.38.uu, ...), custom_call_target="tpu_custom_call" | custom-call | flops 6643777536 | bytes 15000000 | tf_op jit(solution)/shard_map/feed/pallas_call | solution.py:660
  196.8 0.0 copy-start
  196.8 22.1 %sum_tp_down.1 = f32[96,2048]{1,0:T(8,128)} custom-call(bf16[4,2,96,2048]{3,2,1,0:T(8,128)(2,1)} %bitcast.29), custom_call_target="tpu_custom_call" | custom-call | tf_op jit(solution)/shard_map/sum_tp_down/pallas_call | solution.py:93
  218.9 1.2 convert_element_type.27
  220.1 0.0 copy-done
  220.1 0.8 add_convert_fusion
  (1 shorter events, 0.0 us)
Async XLA Ops:
  0.0 8.9 %copy-start.3 = (bf16[768,128]{1,0:T(8,128)(2,1)S(1)}, bf16[768,128]{1,0:T(8,128)(2,1)}, u32[]{:S(2)}) copy-start(bf16[768,128]{1,0:T(8,128)(2,1)} %param.23) | copy-start | bytes 589828
  0.0 8.9 %copy-start.4 = (bf16[768,128]{1,0:T(8,128)(2,1)S(1)}, bf16[768,128]{1,0:T(8,128)(2,1)}, u32[]{:S(2)}) copy-start(bf16[768,128]{1,0:T(8,128)(2,1)} %param.19) | copy-start | bytes 589828
  6.8 42.8 %copy-start.5 = (bf16[32,128,1]{1,0,2:T(8,128)(2,1)S(1)}, bf16[32,128,1]{1,0,2:T(8,128)(2,1)}, u32[]{:S(2)}) copy-start(bf16[32,128,1]{1,0,2:T(8,128)(2,1)} %constant.14) | copy-start | bytes 24580
  104.6 30.7 %copy-start.1 = (bf16[128,2048]{1,0:T(8,128)(2,1)S(1)}, bf16[128,2048]{1,0:T(8,128)(2,1)}, u32[]{:S(2)}) copy-start(bf16[128,2048]{1,0:T(8,128)(2,1)} %param.26) | copy-start | bytes 1572868
  104.6 30.7 %copy-start.2 = (bf16[128,2048]{1,0:T(8,128)(2,1)S(1)}, bf16[128,2048]{1,0:T(8,128)(2,1)}, u32[]{:S(2)}) copy-start(bf16[128,2048]{1,0:T(8,128)(2,1)} %param.25) | copy-start | bytes 1572868
  196.8 23.3 %copy-start = (f32[96,2048]{1,0:T(8,128)S(1)}, f32[96,2048]{1,0:T(8,128)}, u32[]{:S(2)}) copy-start(f32[96,2048]{1,0:T(8,128)} %get-tuple-element.35) | copy-start | bytes 2359300

commit v5 on v4

--- a/solution.py
+++ b/solution.py
@@ -348,20 +348,21 @@
     return t // 2, t % 2
 
 
-def tp_sum_kernel(terms, out, other, parts, relay, arrived, send_sems, recv_sems):
+def tp_sum_kernel(terms, stream, out, other, parts, relay, arrived, send_sems, recv_sems):
     y, core = tp_place()
     ys, mate = y_neighbours(), sibling()
     greet((*ys, mate))
     copies = Copies(send_sems, recv_sems)
     ring = RingSum(copies, parts, relay, arrived, y, *ys, 96)
     own = pair_sum(copies, terms, other, ring, y, core, mate)
-    out[...] = ring.finish(own)
+    summed = ring.finish(own).astype(jnp.bfloat16).astype(jnp.float32)
+    out[...] = (stream[...] + summed).astype(jnp.bfloat16)
     copies.drain_sends()
 
 
 def middle_kernel(
-    terms, residual, gain, d1, d2, g1, u1, stream, whole, dd1, dd2, gg, uu, other, parts, relay, arrived, own,
-    send_sems, recv_sems,
+    mixed, out_small, out_large, residual, gain, d1, d2, g1, u1, stream, whole, dd1, dd2, gg, uu, other, parts,
+    relay, arrived, own, terms, send_sems, recv_sems,
 ):
     z, x = sp_coords()
     y, core = tp_place()
@@ -379,6 +380,12 @@
     ring = RingSum(copies, parts, relay, arrived, y, *ys, 96)
     for job in early + late:
         job.start()
+    turned = (((0,), (0,)), ((), ()))
+    for n in range(2):
+        part = lax.dot_general(
+            mixed[n, 0:128], out_small[...], turned, preferred_element_type=jnp.float32
+        ) + lax.dot_general(mixed[n, 128:256], out_large[...], turned, preferred_element_type=jnp.float32)
+        terms[2 * n : 2 * n + 2] = part.astype(jnp.bfloat16).reshape(2, 2, *residual.shape)
     total = pair_sum(copies, terms, other, ring, y, core, mate)
     for job in early:
         job.pass_on()
@@ -447,9 +454,19 @@
     return value.astype(jnp.bfloat16)
 
 
-def attend_kernel(qa_ref, qb_ref, k_ref, ext_ref, v_ref, o_ref, tot_ref, work_ref, rhs_ref):
+def attend_kernel(
+    qa_ref, qb_ref, k_ref, off_ref, spread_ref, v_ref, o_ref, tot_ref, work_ref, rhs_ref, ext_ref,
+    wide_ref,
+):
     z, x = sp_coords()
     kb = pl.program_id(0)
+
+    wide_ref[...] = lax.dot_general(
+        off_ref[0], spread_ref[...], (((0,), (0,)), ((), ())), preferred_element_type=jnp.float32
+    )
+    for j in range(0, STRIPE, 2):
+        pair = [eight_keys(wide_ref, j), eight_keys(wide_ref, j + 1)]
+        ext_ref[j * 8 : j * 8 + 16, :] = jnp.concatenate(pair, axis=0).astype(jnp.bfloat16)
 
     @pl.when(kb == 0)
     def _():
@@ -480,7 +497,7 @@
                 for c in reversed(range(BLOCK // chunk)):
                     span = slice(c * chunk, (c + 1) * chunk)
                     lhs = jnp.concatenate(
-                        [k_ref[0, span, key_column : key_column + 128], ext_ref[0, span, :]], axis=1
+                        [k_ref[0, span, key_column : key_column + 128], ext_ref[span, :]], axis=1
                     )
                     logit = jnp.dot(lhs, rhs, preferred_element_type=jnp.float32)
                     loss = jnp.maximum(
@@ -537,7 +554,7 @@
         lax.fori_loop(0, 6, body, 0)
 
 
-def attend(qa, qb, k_all, ext, v_all):
+def attend(qa, qb, k_all, off_all, spread, v_all):
     return pl.pallas_call(
         attend_kernel,
         grid=(4,),
@@ -545,7 +562,8 @@
             pl.BlockSpec((4, 256, HALF), lambda kb: (0, 0, 0)),
             pl.BlockSpec((4, 256, HALF), lambda kb: (0, 0, 0)),
             pl.BlockSpec((1, BLOCK, 256), lambda kb: (kb, 0, 0)),
-            pl.BlockSpec((1, BLOCK, 128), lambda kb: (kb, 0, 0)),
+            pl.BlockSpec((1, 32, BLOCK), lambda kb: (kb, 0, 0)),
+            pl.BlockSpec((32, 128), lambda kb: (0, 0)),
             pl.BlockSpec((1, 256, BLOCK), lambda kb: (kb, 0, 0)),
         ],
         out_specs=[
@@ -559,6 +577,8 @@
         scratch_shapes=[
             pltpu.VMEM((BLOCK, TILE), jnp.float32),
             pltpu.VMEM((3, 256, TILE), jnp.bfloat16),
+            pltpu.VMEM((BLOCK, 128), jnp.bfloat16),
+            pltpu.VMEM((BLOCK, 128), jnp.float32),
         ],
         compiler_params=pltpu.CompilerParams(
             dimension_semantics=("arbitrary",), vmem_limit_bytes=VMEM_LIMIT
@@ -567,7 +587,7 @@
             flops=100_000_000_000, bytes_accessed=12_000_000, transcendentals=130_000_000
         ),
         name="attend",
-    )(qa, qb, k_all, ext, v_all)
+    )(qa, qb, k_all, off_all, spread, v_all)
 
 
 def sum_scratch(shape):
@@ -580,16 +600,16 @@
     ]
 
 
-def tp_sum(terms, collective_id, name):
+def tp_sum(terms, stream, collective_id, name):
     shape = (96, terms.shape[-1])
     return comm_call(
         tp_sum_kernel,
-        [(shape, jnp.float32, vmem())],
+        [(shape, jnp.bfloat16, vmem())],
         sum_scratch(shape),
         10,
         collective_id,
         name,
-        [(terms.reshape(4, 2, *shape), vmem())],
+        [(terms.reshape(4, 2, *shape), vmem()), (stream, vmem())],
     )[0]
 
 
@@ -679,12 +699,43 @@
     )(rows, *weights)
 
 
-def rounded(value):
-    return lax.optimization_barrier(value.astype(jnp.bfloat16)).astype(jnp.float32)
-
-
-def striped(value):
-    return value.reshape(STRIPES, STRIPE, -1).swapaxes(0, 1).reshape(BLOCK, -1)
+def eight_keys(ref, j):
+    return ref[pl.ds(j, STRIPES, stride=STRIPE), :]
+
+
+def prepare_kernel(qs, ks, vs, ql, kl, vl, q_own, q_give, key, value, wide, turned):
+    f32, bf16 = jnp.float32, jnp.bfloat16
+    for n, (q, depth) in enumerate(((qs, SMALL_DIM), (ql, LARGE_DIM))):
+        rows = slice(n * 128, (n + 1) * 128)
+        flipped = (q[...].astype(f32) * float(np.float32(LOG2E * depth**-0.5))).T.astype(bf16)
+        q_own[rows, :] = flipped[:, :HALF]
+        q_give[rows, :] = flipped[:, HALF:]
+    for n, (k, v) in enumerate(((ks, vs), (kl, vl))):
+        columns = slice(n * 128, (n + 1) * 128)
+        wide[2 * n] = k[...].astype(f32)
+        wide[2 * n + 1] = v[...].astype(f32)
+        for j in range(0, STRIPE, 2):
+            pair = [eight_keys(wide.at[2 * n], j), eight_keys(wide.at[2 * n], j + 1)]
+            key[j * 8 : j * 8 + 16, columns] = jnp.concatenate(pair, axis=0).astype(bf16)
+            for i in (j, j + 1):
+                turned[n, i * 8 : i * 8 + 8, :] = eight_keys(wide.at[2 * n + 1], i)
+        value[columns, :] = turned[n].T.astype(bf16)
+
+
+def prepare(*arrays):
+    bf16 = jnp.bfloat16
+    shapes = ((256, HALF), (256, HALF), (BLOCK, 256), (256, BLOCK))
+    return pl.pallas_call(
+        prepare_kernel,
+        out_shape=[jax.ShapeDtypeStruct(shape, bf16) for shape in shapes],
+        in_specs=[vmem()] * 6,
+        out_specs=[vmem()] * 4,
+        scratch_shapes=[
+            pltpu.VMEM((4, BLOCK, 128), jnp.float32),
+            pltpu.VMEM((2, BLOCK, 128), jnp.float32),
+        ],
+        name="prepare",
+    )(*arrays)
 
 
 def on_device(
@@ -692,15 +743,10 @@
     out_small, out_large, residual, norm_gain, gate_weight, up_weight, down_weight,
 ):
     f32, bf16 = jnp.float32, jnp.bfloat16
-    scales = np.concatenate(
-        [np.full(128, LOG2E * SMALL_DIM**-0.5), np.full(128, LOG2E * LARGE_DIM**-0.5)]
-    ).astype(np.float32)
-    query = jnp.concatenate([query_small, query_large], axis=1).astype(f32) * scales
-    query = query.astype(bf16).T
-    key = striped(jnp.concatenate([key_small, key_large], axis=1))
-    value = striped(jnp.concatenate([value_small, value_large], axis=1)).T
+    q_own, q_give, key, value = prepare(
+        query_small, key_small, value_small, query_large, key_large, value_large
+    )
     offsets = jnp.concatenate([offset_small, offset_large], axis=0)
-    offsets = offsets.reshape(3, STRIPES, STRIPE).swapaxes(1, 2).reshape(3, BLOCK)
     offsets = jnp.pad(offsets, ((0, 29), (0, 0)))
     gate, up, down = gate_weight.T, up_weight.T, down_weight
     units = down.shape[0]
@@ -719,15 +765,12 @@
         43,
         0,
         "gather_qkv",
-        [(array, vmem()) for array in (query[:, :HALF], query[:, HALF:], key, value, offsets, gate, down)],
+        [(array, vmem()) for array in (q_own, q_give, key, value, offsets, gate, down)],
     )
     spread = np.zeros((32, 128), np.float32)
     for head in range(3):
         spread[head, 3 * head : 3 * head + 3] = 1
-    ext = jnp.einsum(
-        "bhs,hc->bsc", off_all, jnp.asarray(spread, bf16), preferred_element_type=f32
-    ).astype(bf16)
-    outs, totals = attend(qa_all, qb_all, k_all, ext, v_all)
+    outs, totals = attend(qa_all, qb_all, k_all, off_all, jnp.asarray(spread, bf16), v_all)
     half = (256, HALF)
     buffers = [pltpu.VMEM((4, 16, 4 * BLOCK), f32), pltpu.VMEM((4, 256, 4 * BLOCK), bf16)]
     for shape in ((4, *half), (2, 128, HALF), (2, *half), half):
@@ -745,10 +788,7 @@
         "mix",
         [(totals, vmem()), (up, vmem()), (down, vmem()), (outs, hbm())],
     )
-    out_weight = jnp.concatenate([out_small, out_large], axis=0)
-    part = jnp.einsum("hct,cd->htd", mixed, out_weight, preferred_element_type=f32)
-    shape = (96, part.shape[-1])
-    terms = part.astype(bf16).reshape(4, 2, *shape)
+    shape = residual.shape
     stream, rows, dd1, dd2, gg, uu = comm_call(
         middle_kernel,
         [
@@ -759,16 +799,18 @@
             ((4, *g1.shape), bf16, hbm()),
             ((4, *u1.shape), bf16, hbm()),
         ],
-        [*sum_scratch(shape), pltpu.VMEM(shape, bf16)],
+        [*sum_scratch(shape), pltpu.VMEM(shape, bf16), pltpu.VMEM((4, 2, *shape), bf16)],
         47,
         3,
         "middle",
-        [(terms, vmem()), (residual, vmem()), (norm_gain.reshape(1, -1), vmem())]
+        [
+            (array, vmem())
+            for array in (mixed, out_small, out_large, residual, norm_gain.astype(f32).reshape(1, -1))
+        ]
         + [(array, hbm()) for array in (d1, d2, g1, u1)],
     )
     down_terms = feed(rows.reshape(BLOCK, 2048), g1, gg, u1, uu, d1, dd1, d2, dd2)
-    summed = tp_sum(down_terms, 5, "sum_tp_down")
-    return (stream + rounded(summed)).astype(bf16)
+    return tp_sum(down_terms, stream, 5, "sum_tp_down")
 
 
 def solution(mesh):

time: 224 us -> 214 us (0.955)
  matrix products: 5.93 us -> 0 us
  local copies, waits for them, and re-layouts: 7.34 us -> 1.77 us
  Pallas kernels: 203 us -> 207 us
    dot_general x2 -> x0, matrix products: 5.93 us -> none  [the longest x1 3.69 us: on_device(): jnp.einsum('hct,cd->htd', mixed, out_weight, preferred_element_type=f32)]
    reshape x6 -> x0, local copies, waits for them, and re-layouts: 3.56 us -> none  [the longest x2 1.9 us: striped(): return value.reshape(STRIPES, STRIPE, -1).swapaxes(0, 1).reshape(BLOCK, -1)]
    pallas_call x0 -> x1, Pallas kernels: none -> 3.12 us  [prepare(): pl.pallas_call(prepare_kernel, out_shape=[jax.ShapeDtypeStruct(shape, bf1...]
where the time goes in v5:
time: 214 us; the launch traced here: 212 us
  Pallas kernels  207 us (97%)
  other arithmetic  2.62 us (1%)
    pallas_call x4, Pallas kernels, comm_call(): pl.pallas_call(kernel, out_shape=[jax.ShapeDtypeStruct(shape, dtype) for...  136 us
    pallas_call x1, Pallas kernels, attend(): pl.pallas_call(attend_kernel, grid=(4,), in_specs=[pl.BlockSpec((4, 256,...  54.5 us
    pallas_call x1, Pallas kernels, feed(): pl.pallas_call(feed_kernel, out_shape=jax.ShapeDtypeStruct((BLOCK, 2048),...  14 us

profile of v5, /device:TPU:96, one launch (start us, length us, event | category | flops | bytes accessed | tf_op | source)
XLA Modules:
  0.0 211.6 jit_solution(7053693698384205555)
XLA Ops:
  0.0 1.3 reshape.15
  1.3 1.3 fusion.2.off
  2.6 3.1 %prepare.1 = (bf16[256,384]{1,0:T(8,128)(2,1)}, bf16[256,384]{1,0:T(8,128)(2,1)}, bf16[768,256]{1,0:T(8,128)(2,1)}, bf16[256,768]{1,0:T(8,128)(2,1)}) custom-call(bf16[768,128]{1,0:T(8,128)(2,1)} %qs.1, bf16[768,128]{1,0:T(8,128)(2,1)} %ks.1, bf16[768,128]{1,0:T(8,128)(2,1)} %vs.1, bf16[768,128]{1,0:T(8,128)(2,1)} %ql.1, bf16[768,128]{1,0:T(8,128)(2,1)} %kl.1, ...), custom_call_target="tpu_custom_call" | custom-call | tf_op jit(solution)/shard_map/prepare/pallas_call | solution.py:728
  5.7 39.6 %gather_qkv.1 = (bf16[4,256,384]{2,1,0:T(8,128)(2,1)}, bf16[4,256,384]{2,1,0:T(8,128)(2,1)}, bf16[4,768,256]{2,1,0:T(8,128)(2,1)}, bf16[4,256,768]{2,1,0:T(8,128...) custom-call(bf16[256,384]{1,0:T(8,128)(2,1)} %get-tuple-element.27.q_own, ...), custom_call_target="tpu_custom_call" | custom-call | tf_op jit(solution)/shard_map/gather_qkv/pallas_call | solution.py:93
  45.3 54.5 %attend.1 = (bf16[4,256,3072]{2,1,0:T(8,128)(2,1)}, f32[16,3072]{1,0:T(8,128)}) custom-call(bf16[4,256,384]{2,1,0:T(8,128)(2,1)} %get-tuple-element.31.qa_ref, bf16[4,256,384]{2,1,0:T(8,128)(2,1)} %get-tuple-element.32.qb_ref, bf16[4,768,256]{2,1,0:T(8,128)(2,1)} %get-tuple-element.33.k_ref, bf16[4,32,768]{2,1,0:T(8,128)(2,1)} %get-tuple-element.34.off_ref, ...), custom_call_target="tpu_custom_call" | custom-call | flops 99999997952 | bytes 12000000 | tf_op jit(solution)/shard_map/attend/pallas_call | solution.py:558
  99.8 30.6 %mix.1 = (bf16[2,256,384]{2,1,0:T(8,128)(2,1)}, bf16[4,704,128]{2,1,0:T(8,128)(2,1)}, bf16[4,352,128]{2,1,0:T(8,128)(2,1)}) custom-call(f32[16,3072]{1,0:T(8,128)} %get-tuple-element.36.tot, bf16[704,128]{1,0:T(8,128)(2,1)} %bitcast.7, bf16[704,128]{1,0:T(8,128)(2,1)} %down.3, bf16[4,256,3072]{2,1,0:T(8,128)(2,1)} %get-tuple-element.37.o_hbm), custom_call_target="tpu_custom_call" | custom-call | tf_op jit(solution)/shard_map/mix/pallas_call | solution.py:93
  130.3 42.7 %middle.1 = (f32[96,2048]{1,0:T(8,128)}, bf16[4,2,96,2048]{3,2,1,0:T(8,128)(2,1)}, bf16[4,4,352,128]{3,2,1,0:T(8,128)(2,1)}, bf16[4,4,352,128]{3,2,1,0:T(8,128)(...) custom-call(bf16[2,256,384]{2,1,0:T(8,128)(2,1)} %get-tuple-element.38.mixed, ...), custom_call_target="tpu_custom_call" | custom-call | tf_op jit(solution)/shard_map/middle/pallas_call | solution.py:93
  173.1 14.0 %feed.1 = bf16[768,2048]{1,0:T(8,128)(2,1)} custom-call(bf16[768,2048]{1,0:T(8,128)(2,1)} %bitcast.9, bf16[4,704,128]{2,1,0:T(8,128)(2,1)} %get-tuple-element.41.g1, bf16[4,4,704,128]{3,2,1,0:T(8,128)(2,1)} %get-tuple-element.44.gg, bf16[4,704,128]{2,1,0:T(8,128)(2,1)} %get-tuple-element.42.u1, bf16[4,4,704,128]{3,2,1,0:T(8,128)(2,1)} %get-tuple-element.45.uu, ...), custom_call_target="tpu_custom_call" | custom-call | flops 6643777536 | bytes 15000000 | tf_op jit(solution)/shard_map/feed/pallas_call | solution.py:680
  187.1 22.7 %sum_tp_down.1 = bf16[96,2048]{1,0:T(8,128)(2,1)} custom-call(bf16[4,2,96,2048]{3,2,1,0:T(8,128)(2,1)} %bitcast.5, f32[96,2048]{1,0:T(8,128)} %get-tuple-element.48.stream), custom_call_target="tpu_custom_call" | custom-call | tf_op jit(solution)/shard_map/sum_tp_down/pallas_call | solution.py:93
  209.8 1.8 copy.18

commit v6 on v5

--- a/solution.py
+++ b/solution.py
@@ -346,18 +346,6 @@
 def tp_place():
     t = lax.axis_index("tp")
     return t // 2, t % 2
-
-
-def tp_sum_kernel(terms, stream, out, other, parts, relay, arrived, send_sems, recv_sems):
-    y, core = tp_place()
-    ys, mate = y_neighbours(), sibling()
-    greet((*ys, mate))
-    copies = Copies(send_sems, recv_sems)
-    ring = RingSum(copies, parts, relay, arrived, y, *ys, 96)
-    own = pair_sum(copies, terms, other, ring, y, core, mate)
-    summed = ring.finish(own).astype(jnp.bfloat16).astype(jnp.float32)
-    out[...] = (stream[...] + summed).astype(jnp.bfloat16)
-    copies.drain_sends()
 
 
 def middle_kernel(
@@ -600,23 +588,16 @@
     ]
 
 
-def tp_sum(terms, stream, collective_id, name):
-    shape = (96, terms.shape[-1])
-    return comm_call(
-        tp_sum_kernel,
-        [(shape, jnp.bfloat16, vmem())],
-        sum_scratch(shape),
-        10,
-        collective_id,
-        name,
-        [(terms.reshape(4, 2, *shape), vmem()), (stream, vmem())],
-    )[0]
-
-
 def feed_kernel(
-    rows, g1, gg, u1, uu, d1, dd1, d2, dd2, out, r_vmem, gate_w, up_w, down_w, gate, hidden, sems
+    rows, g1, gg, u1, uu, d1, dd1, d2, dd2, out, r_vmem, gate_w, up_w, down_w, gate, hidden, terms, other, parts,
+    relay, arrived, sems, send_sems, recv_sems,
 ):
     z, x = sp_coords()
+    y, core = tp_place()
+    ys, mate = y_neighbours(), sibling()
+    greet((*ys, mate))
+    copies = Copies(send_sems, recv_sems)
+    ring = RingSum(copies, parts, relay, arrived, y, *ys, 96)
     half = d1.shape[1]
     row_copy = pltpu.make_async_copy(rows, r_vmem, sems.at[64])
     row_copy.start()
@@ -666,37 +647,54 @@
     for copy in waits[2]:
         copy.wait()
 
-    def lower(span):
-        out[span, :] = jnp.dot(
-            hidden[span, :], down_w[...], preferred_element_type=jnp.float32
-        ).astype(jnp.bfloat16)
-
-    over_rows(lower)
+    order = (ring.far, ring.after, ring.before, y)
+    sends = (ring.send_far, ring.send_after, ring.send_before)
+    given = []
+
+    def add(n):
+        given[n].wait_recv()
+        parts[order[n]] = plus(terms[order[n], core], other[order[n]])
+        sends[n]()
+
+    for n, place in enumerate(order):
+        span = pl.ds(pl.multiple_of(place * 192, 64), 192)
+        down = jnp.dot(hidden[span, :], down_w[...], preferred_element_type=jnp.float32)
+        terms[place] = down.astype(jnp.bfloat16).reshape(2, 96, 2048)
+        copy = copies.make(terms.at[place, 1 - core], other.at[place], mate)
+        copy.start()
+        given.append(copy)
+        if n:
+            add(n - 1)
+    ring.pass_on()
+    given[3].wait_recv()
+    own = terms[y, core].astype(jnp.float32) + other[y].astype(jnp.float32)
+    out[...] = ring.finish(own).astype(jnp.bfloat16)
+    copies.drain_sends()
 
 
 def feed(rows, *weights):
     units = weights[0].shape[1]
     bf16 = jnp.bfloat16
-    return pl.pallas_call(
+    shape = (96, 2048)
+    return comm_call(
         feed_kernel,
-        out_shape=jax.ShapeDtypeStruct((BLOCK, 2048), bf16),
-        in_specs=[hbm()] * (1 + len(weights)),
-        out_specs=vmem(),
-        scratch_shapes=[
+        [(shape, bf16, vmem())],
+        [
             pltpu.VMEM((BLOCK, 2048), bf16),
             pltpu.VMEM((units, 2048), bf16),
             pltpu.VMEM((units, 2048), bf16),
             pltpu.VMEM((units, 2048), bf16),
             pltpu.VMEM((BLOCK, units), jnp.float32),
             pltpu.VMEM((BLOCK, units), bf16),
+            pltpu.VMEM((4, 2, *shape), bf16),
+            *sum_scratch(shape),
             pltpu.SemaphoreType.DMA((65,)),
         ],
-        compiler_params=pltpu.CompilerParams(vmem_limit_bytes=VMEM_LIMIT),
-        cost_estimate=pl.CostEstimate(
-            flops=6 * BLOCK * 2048 * units, bytes_accessed=15_000_000, transcendentals=BLOCK * units
-        ),
-        name="feed",
-    )(rows, *weights)
+        10,
+        5,
+        "feed",
+        [(array, hbm()) for array in (rows, *weights)],
+    )[0]
 
 
 def eight_keys(ref, j):
@@ -809,8 +807,8 @@
         ]
         + [(array, hbm()) for array in (d1, d2, g1, u1)],
     )
-    down_terms = feed(rows.reshape(BLOCK, 2048), g1, gg, u1, uu, d1, dd1, d2, dd2)
-    return tp_sum(down_terms, stream, 5, "sum_tp_down")
+    summed = feed(rows.reshape(BLOCK, 2048), g1, gg, u1, uu, d1, dd1, d2, dd2)
+    return (stream + summed.astype(f32)).astype(bf16)
 
 
 def solution(mesh):

time: 214 us -> 209 us (0.977)
  Pallas kernels: 207 us -> 201 us
    pallas_call x1 -> x0, Pallas kernels: 14 us -> none  [feed(): pl.pallas_call(feed_kernel, out_shape=jax.ShapeDtypeStruct((BLOCK, 2048),...]
    pallas_call x4, Pallas kernels: 136 us -> 144 us  [comm_call(): pl.pallas_call(kernel, out_shape=[jax.ShapeDtypeStruct(shape, dtype) for...]
where the time goes in v6:
time: 209 us; the launch traced here: 206 us
  Pallas kernels  201 us (96%)
  other arithmetic  4.43 us (2%)
    pallas_call x4, Pallas kernels, comm_call(): pl.pallas_call(kernel, out_shape=[jax.ShapeDtypeStruct(shape, dtype) for...  144 us
    pallas_call x1, Pallas kernels, attend(): pl.pallas_call(attend_kernel, grid=(4,), in_specs=[pl.BlockSpec((4, 256,...  54.4 us

profile of v6, /device:TPU:96, one launch (start us, length us, event | category | flops | bytes accessed | tf_op | source)
XLA Modules:
  0.0 205.8 jit_solution(1046105095825175876)
XLA Ops:
  0.0 1.3 reshape.11
  1.3 1.3 fusion.2.off
  2.6 3.1 %prepare.1 = (bf16[256,384]{1,0:T(8,128)(2,1)}, bf16[256,384]{1,0:T(8,128)(2,1)}, bf16[768,256]{1,0:T(8,128)(2,1)}, bf16[256,768]{1,0:T(8,128)(2,1)}) custom-call(bf16[768,128]{1,0:T(8,128)(2,1)} %qs.1, bf16[768,128]{1,0:T(8,128)(2,1)} %ks.1, bf16[768,128]{1,0:T(8,128)(2,1)} %vs.1, bf16[768,128]{1,0:T(8,128)(2,1)} %ql.1, bf16[768,128]{1,0:T(8,128)(2,1)} %kl.1, ...), custom_call_target="tpu_custom_call" | custom-call | tf_op jit(solution)/shard_map/prepare/pallas_call | solution.py:726
  5.7 39.5 %gather_qkv.1 = (bf16[4,256,384]{2,1,0:T(8,128)(2,1)}, bf16[4,256,384]{2,1,0:T(8,128)(2,1)}, bf16[4,768,256]{2,1,0:T(8,128)(2,1)}, bf16[4,256,768]{2,1,0:T(8,128...) custom-call(bf16[256,384]{1,0:T(8,128)(2,1)} %get-tuple-element.27.q_own, ...), custom_call_target="tpu_custom_call" | custom-call | tf_op jit(solution)/shard_map/gather_qkv/pallas_call | solution.py:93
  45.3 54.4 %attend.1 = (bf16[4,256,3072]{2,1,0:T(8,128)(2,1)}, f32[16,3072]{1,0:T(8,128)}) custom-call(bf16[4,256,384]{2,1,0:T(8,128)(2,1)} %get-tuple-element.31.qa_ref, bf16[4,256,384]{2,1,0:T(8,128)(2,1)} %get-tuple-element.32.qb_ref, bf16[4,768,256]{2,1,0:T(8,128)(2,1)} %get-tuple-element.33.k_ref, bf16[4,32,768]{2,1,0:T(8,128)(2,1)} %get-tuple-element.34.off_ref, ...), custom_call_target="tpu_custom_call" | custom-call | flops 99999997952 | bytes 12000000 | tf_op jit(solution)/shard_map/attend/pallas_call | solution.py:546
  99.7 30.5 %mix.1 = (bf16[2,256,384]{2,1,0:T(8,128)(2,1)}, bf16[4,704,128]{2,1,0:T(8,128)(2,1)}, bf16[4,352,128]{2,1,0:T(8,128)(2,1)}) custom-call(f32[16,3072]{1,0:T(8,128)} %get-tuple-element.36.tot, bf16[704,128]{1,0:T(8,128)(2,1)} %bitcast.6, bf16[704,128]{1,0:T(8,128)(2,1)} %down.3, bf16[4,256,3072]{2,1,0:T(8,128)(2,1)} %get-tuple-element.37.o_hbm), custom_call_target="tpu_custom_call" | custom-call | tf_op jit(solution)/shard_map/mix/pallas_call | solution.py:93
  130.2 42.7 %middle.1 = (f32[96,2048]{1,0:T(8,128)}, bf16[4,2,96,2048]{3,2,1,0:T(8,128)(2,1)}, bf16[4,4,352,128]{3,2,1,0:T(8,128)(2,1)}, bf16[4,4,352,128]{3,2,1,0:T(8,128)(...) custom-call(bf16[2,256,384]{2,1,0:T(8,128)(2,1)} %get-tuple-element.38.mixed, ...), custom_call_target="tpu_custom_call" | custom-call | tf_op jit(solution)/shard_map/middle/pallas_call | solution.py:93
  173.0 0.0 copy-start
  173.0 31.0 %feed.1 = bf16[96,2048]{1,0:T(8,128)(2,1)} custom-call(bf16[768,2048]{1,0:T(8,128)(2,1)} %bitcast.4, bf16[4,704,128]{2,1,0:T(8,128)(2,1)} %get-tuple-element.41.g1, bf16[4,4,704,128]{3,2,1,0:T(8,128)(2,1)} %get-tuple-element.45.gg, bf16[4,704,128]{2,1,0:T(8,128)(2,1)} %get-tuple-element.42.u1, bf16[4,4,704,128]{3,2,1,0:T(8,128)(2,1)} %get-tuple-element.46.uu, ...), custom_call_target="tpu_custom_call" | custom-call | tf_op jit(solution)/shard_map/feed/pallas_call | solution.py:93
  203.9 0.0 copy-done
  204.0 1.8 add_convert_fusion
Async XLA Ops:
  173.0 31.0 %copy-start = (f32[96,2048]{1,0:T(8,128)S(1)}, f32[96,2048]{1,0:T(8,128)}, u32[]{:S(2)}) copy-start(f32[96,2048]{1,0:T(8,128)} %get-tuple-element.43) | copy-start | bytes 2359300
